TPU v7x, 256 devices: a whole 4x4x8 slice. The times are simulated.
256 devices in a mesh: sp: 64 (over z, y, core), tp: 4 (over x).
Axes of the slice: x: 4, y: 4, z: 8, core: 2. Of those that a mesh axis runs over, the one named last changes fastest.
Arguments:
- stream_in: bfloat16 [49152, 2048], P(('sp', 'tp')), may hold values from -6 to 6
- query_wide: bfloat16 [49152, 512], P('sp', 'tp'), may hold values from -6 to 6
- key_wide: bfloat16 [49152, 512], P('sp', 'tp'), may hold values from -6 to 6
- value_wide: bfloat16 [49152, 512], P('sp', 'tp'), may hold values from -6 to 6
- gate_wide: bfloat16 [49152, 512], P('sp', 'tp'), may hold values from -6 to 6
- decay_wide: float32 [4, 49152], P('tp', 'sp'), may hold values from -2.3 to 0, as said below
- query_narrow: bfloat16 [49152, 512], P('sp', 'tp'), may hold values from -6 to 6
- key_narrow: bfloat16 [49152, 512], P('sp', 'tp'), may hold values from -6 to 6
- value_narrow: bfloat16 [49152, 512], P('sp', 'tp'), may hold values from -6 to 6
- gate_narrow: bfloat16 [49152, 512], P('sp', 'tp'), may hold values from -6 to 6
- decay_narrow: float32 [8, 49152], P('tp', 'sp'), may hold values from -2.3 to 0, as said below
- output_wide: bfloat16 [512, 2048], P('tp'), may hold values from -0.25 to 0.25
- output_narrow: bfloat16 [512, 2048], P('tp'), may hold values from -0.25 to 0.25
- norm_gain: bfloat16 [2048], replicated, may hold values from 0.099609375 to 1.8984375
- up_weight: bfloat16 [2048, 8192], P('sp', 'tp'), may hold values from -0.125 to 0.125
- down_weight: bfloat16 [8192, 2048], P('tp', 'sp'), may hold values from -0.0625 to 0.0625
Outputs:
- layer_out: bfloat16 [49152, 2048], P(('sp', 'tp'))
Inputs may be any that keep to these rules, and one draw needn't show every extreme that they name: `decay_wide`: each entry is the logarithm of one head's retention factor at one position. `decay_narrow`: each entry is the logarithm of one head's retention factor at one position.
All inputs are finite; a program needn't handle non-finite values.
Results may differ from a plain program's by a relative error of at most 0.02.
Values may be sent and summed in bfloat16 or wider, within the bound.
A program may use at most 128 MiB of HBM per device.

v0:
```python
import jax
import jax.numpy as jnp
from jax import lax
from jax.sharding import Mesh
from jax.sharding import PartitionSpec as P

HDW = 128
HDN = 64
BLOCK = 128
SP = ("sp_0", "sp_1", "sp_2")
SP_TP = ("sp_0", "sp_1", "sp_2", "tp")


head_eps = 1e-05
norm_eps = 1e-06
rope_base = 10000.0


def rows_first(arrays, axis, dims):
    turned = [jnp.moveaxis(a, dim, 0) for a, dim in zip(arrays, dims)]
    both = jnp.concatenate([t.reshape(len(t), -1) for t in turned], axis=1)
    out, at, finished = (lax.all_gather(both, axis, axis=0, tiled=True), 0, [])
    for t, dim in zip(turned, dims):
        section = out[:, at : at + t[0].size].reshape(-1, *t.shape[1:])
        finished.append(jnp.moveaxis(section, 0, dim))
        at += t[0].size
    return tuple(finished)


def nothing_yet(shard, identity):
    return jax.tree.map(
        lambda part, zero: jnp.zeros_like(part) + jnp.asarray(zero, part.dtype), shard, identity
    )


def gathered_once(shard, axis):
    leaves = jax.tree.leaves(shard)
    sequence = sorted(range(len(leaves)), key=lambda k: -leaves[k].size)
    width = (1, *leaves[sequence[0]].shape)[-1]
    lines = [
        jnp.pad(leaves[k].reshape(-1), (0, -leaves[k].size % width)).reshape(-1, width)
        for k in sequence
    ]
    both, at, found = (lax.all_gather(jnp.concatenate(lines), axis), 0, {})
    for k, line in zip(sequence, lines):
        section = both[:, at : at + len(line)].reshape(len(both), -1)
        found[k] = section[:, : leaves[k].size].reshape(-1, *leaves[k].shape)
        at += len(line)
    numbers = iter(range(len(leaves)))
    return jax.tree.map(lambda _: found[next(numbers)], shard)


def entering(shard, axes, combine, identity):
    before = start = nothing_yet(shard, identity)
    so_far = shard
    for axis in reversed(axes):
        length, mine = (lax.axis_size(axis), lax.axis_index(axis))
        pieces = gathered_once(
            jax.tree.map(
                lambda part, kind: part.astype(kind),
                so_far,
                (jnp.bfloat16, jnp.bfloat16, jnp.bfloat16, jnp.bfloat16),
            ),
            axis,
        )
        inside, so_far = (start, start)
        for k in range(length):
            passed = k < mine
            so_far = combine(
                so_far, jax.tree.map(lambda part, own: part[k].astype(own.dtype), pieces, shard)
            )
            inside = jax.tree.map(lambda new, old: jnp.where(passed, new, old), so_far, inside)
        before = combine(inside, before)
    return before


def in_blocks(shard, dim, length):
    before, after = (shard.shape[:dim], shard.shape[dim + 1 :])
    return jnp.moveaxis(shard.reshape(*before, length, -1, *after), dim, 0)


def sum_at_owner(shard, axis, dim):
    tiles = in_blocks(shard, dim, lax.axis_size(axis))
    arrived = lax.all_to_all(tiles, axis, split_axis=0, concat_axis=0, tiled=True)
    return arrived.astype(jnp.float32).sum(axis=0)


def rotate(values, places):
    half = values.shape[-1] // 2
    inverse = rope_base ** (-jnp.arange(half, dtype=jnp.float32) / half)
    angles = places[:, None] * inverse[None, :]
    cosine = jnp.cos(angles)[:, None, :]
    sine = jnp.sin(angles)[:, None, :]
    front = values[..., :half]
    back = values[..., half:]
    return jnp.concatenate([front * cosine - back * sine, back * cosine + front * sine], axis=-1)


def block_step(carried, inputs):
    query, keys, values, log_rate = inputs
    running = jnp.cumsum(log_rate, axis=0)
    spread = running[:, None, :] - running[None, :, :]
    length = log_rate.shape[0]
    lower = (jnp.arange(length)[:, None] >= jnp.arange(length)[None, :])[:, :, None]
    factor = jnp.where(lower, jnp.exp(jnp.minimum(spread, 0.0)), 0.0)
    scores = jnp.einsum("thd,shd->tsh", query, keys) * factor
    within = jnp.einsum("tsh,she->the", scores, values)
    across = jnp.einsum("thd,hde->the", query, carried) * jnp.exp(running)[:, :, None]
    tail_decay = jnp.exp(running[-1][None, :] - running)
    updated = jnp.exp(running[-1])[:, None, None] * carried + jnp.einsum(
        "shd,she->hde", keys * tail_decay[:, :, None], values
    )
    return (updated, within + across)


def head_norm(values):
    centre = values - jnp.mean(values, axis=-1, keepdims=True)
    spread = jnp.mean(centre * centre, axis=-1, keepdims=True)
    return centre * lax.rsqrt(spread + head_eps)


def local_group(query, keys, values, log_rate, width, places):
    length = query.shape[0]
    count_of_heads = query.shape[1] // width
    blocks = length // BLOCK

    def split(array):
        return array.astype(jnp.float32).reshape(length, count_of_heads, width)

    query_rot = rotate(split(query), places)
    keys_rot = rotate(split(keys), places) * width ** (-0.5)
    rates = log_rate.T
    carried = jnp.zeros((count_of_heads, width, width), jnp.float32)
    final_state, outputs = lax.scan(
        block_step,
        carried,
        (
            query_rot.reshape(blocks, BLOCK, count_of_heads, width),
            keys_rot.reshape(blocks, BLOCK, count_of_heads, width),
            split(values).reshape(blocks, BLOCK, count_of_heads, width),
            rates.reshape(blocks, BLOCK, count_of_heads),
        ),
    )
    running = jnp.cumsum(rates, axis=0)
    return (
        query_rot,
        outputs.reshape(length, count_of_heads, width),
        final_state,
        jnp.exp(running[-1]),
        running,
    )


def finish_group(query_rot, outputs, incoming, running, gate):
    length = outputs.shape[0]
    outputs = (
        outputs + jnp.einsum("thd,hde->the", query_rot, incoming) * jnp.exp(running)[:, :, None]
    )
    normed = head_norm(outputs).reshape(length, -1)
    return (jax.nn.silu(gate.astype(jnp.float32)) * normed).astype(jnp.bfloat16)


def chain(earlier, later):
    rate_wide, memory_wide, rate_narrow, memory_narrow = earlier
    later_rate_wide, later_memory_wide, later_rate_narrow, later_memory_narrow = later
    return (
        rate_wide * later_rate_wide,
        memory_wide * later_rate_wide[:, None, None] + later_memory_wide,
        rate_narrow * later_rate_narrow,
        memory_narrow * later_rate_narrow[:, None, None] + later_memory_narrow,
    )


def row_norm(middle, norm_gain):
    middle_f = middle.astype(jnp.float32)
    scale = lax.rsqrt(jnp.mean(middle_f * middle_f, axis=-1, keepdims=True) + norm_eps)
    return (middle_f * scale * norm_gain.astype(jnp.float32)).astype(jnp.bfloat16)


def on_device(
    stream_in,
    query_wide,
    key_wide,
    value_wide,
    gate_wide,
    decay_wide,
    query_narrow,
    key_narrow,
    value_narrow,
    gate_narrow,
    decay_narrow,
    output_wide,
    output_narrow,
    norm_gain,
    up_weight,
    down_weight,
):
    length = query_wide.shape[0]
    up_full, down_full = rows_first((up_weight, down_weight), SP, (0, 1))
    places = (lax.axis_index(SP) * length + jnp.arange(length, dtype=jnp.int32)).astype(jnp.float32)
    wide_query, wide_out, wide_state, wide_total, wide_running = local_group(
        query_wide, key_wide, value_wide, decay_wide, HDW, places
    )
    narrow_query, narrow_out, narrow_state, narrow_total, narrow_running = local_group(
        query_narrow, key_narrow, value_narrow, decay_narrow, HDN, places
    )
    identity = (
        jnp.ones_like(wide_total),
        jnp.zeros_like(wide_state),
        jnp.ones_like(narrow_total),
        jnp.zeros_like(narrow_state),
    )
    incoming = entering((wide_total, wide_state, narrow_total, narrow_state), SP, chain, identity)
    mixed_wide = finish_group(wide_query, wide_out, incoming[1], wide_running, gate_wide)
    mixed_narrow = finish_group(narrow_query, narrow_out, incoming[3], narrow_running, gate_narrow)
    mixed_sum = sum_at_owner(
        (
            jnp.dot(mixed_wide, output_wide, preferred_element_type=jnp.float32)
            + jnp.dot(mixed_narrow, output_narrow, preferred_element_type=jnp.float32)
        ).astype(jnp.bfloat16),
        "tp",
        0,
    )
    middle = (stream_in.astype(jnp.float32) + mixed_sum).astype(jnp.bfloat16)
    normed = lax.all_gather(row_norm(middle, norm_gain), "tp", axis=0, tiled=True)
    up_sum = jnp.dot(normed, up_full, preferred_element_type=jnp.float32)
    hidden = jnp.square(jax.nn.relu(up_sum)).astype(jnp.bfloat16)
    down_sum = jnp.dot(hidden, down_full, preferred_element_type=jnp.float32)
    down_rows = lax.psum_scatter(
        down_sum.astype(jnp.bfloat16), "tp", scatter_dimension=0, tiled=True
    ).astype(jnp.float32)
    return (middle.astype(jnp.float32) + down_rows).astype(jnp.bfloat16)


def solution(mesh):
    split = Mesh(mesh.devices.reshape(8, 4, 2, mesh.shape["tp"]), ("sp_0", "sp_1", "sp_2", "tp"))
    in_specs = (
        P(SP_TP, None),
        P(SP, "tp"),
        P(SP, "tp"),
        P(SP, "tp"),
        P(SP, "tp"),
        P("tp", SP),
        P(SP, "tp"),
        P(SP, "tp"),
        P(SP, "tp"),
        P(SP, "tp"),
        P("tp", SP),
        P("tp", None),
        P("tp", None),
        P(),
        P(SP, "tp"),
        P("tp", SP),
    )
    out_specs = P(SP_TP, None)
    return jax.shard_map(
        on_device, mesh=split, in_specs=in_specs, out_specs=out_specs, check_vma=False
    )
```

profile of v0, /device:TPU:1, one launch (start us, length us, event | category | flops | bytes accessed | tf_op | source)
XLA Modules:
  0.0 398.5 jit_solution(7533716243381743910)
XLA Ops:
  6.6 1.1 copy.156
  7.8 1.1 copy.158
  10.4 25.0 %while.27 = (s32[]{:T(128)}, f32[2,64,64]{2,1,0:T(8,128)S(1)}, f32[6,128,2,64]{1,0,3,2:T(8,128)}, f32[6,128,2]{2,1,0:T(8,128)S(1)}, f32[6,128,2,64]{1,0,3,2:T(8,...) while((s32[]{:T(128)}, f32[2,64,64]{2,1,0:T(8,128)S(1)}, ...), condition=%wide.region_5.6_spmd.clone, body=%wide.region_3.5_spmd.clone.sunk | while | flops 12877827 | bytes 1099440 | solution.py:134
  11.5 2.8 dynamic_update_slice.14
  15.7 2.8 dynamic_update_slice.14
  19.9 2.8 dynamic_update_slice.14
  24.0 2.8 dynamic_update_slice.14
  28.2 2.8 dynamic_update_slice.14
  32.3 2.8 dynamic_update_slice.14
  35.5 1.0 reshape_reshape.22
  36.5 1.9 fusion.88
  38.6 0.9 maximum_multiply_fusion.1
  39.5 22.9 %while.26 = (s32[]{:T(128)}, f32[1,128,128]{2,1,0:T(8,128)S(1)}, f32[6,128,1,128]{3,1,0,2:T(8,128)}, f32[6,128,1]{1,2,0:T(1,128)S(1)}, f32[6,128,1,128]{3,2,1,0:...) while((s32[]{:T(128)}, f32[1,128,128]{2,1,0:T(8,128)S(1)}, ...), condition=%wide.region_2.3_spmd.clone, body=%wide.region_0.2_spmd.clone.sunk | while | flops 17006596 | bytes 1515172 | solution.py:134
  41.9 0.6 constant_dynamic-update-slice_fusion.2
  44.3 0.6 fusion.342
  45.7 0.6 constant_dynamic-update-slice_fusion.2
  48.1 0.6 fusion.342
  49.6 0.6 constant_dynamic-update-slice_fusion.2
  53.4 0.6 constant_dynamic-update-slice_fusion.2
  57.2 0.6 constant_dynamic-update-slice_fusion.2
  61.0 0.6 constant_dynamic-update-slice_fusion.2
  63.2 0.6 slice.432
  63.8 0.7 slice.431
  65.8 0.6 reduce-window.14
  67.1 4.7 %all-gather.3 = bf16[2,194,128]{2,1,0:T(8,128)(2,1)S(1)} all-gather(bf16[1,194,128]{2,1,0:T(8,128)(2,1)S(1)} %maximum_bitcast_fusion), channel_id=2, replica_groups=mesh['sp_0'=8,'sp_1'=4,'sp_2'=2,'tp'=4] {'sp_2'}, dimensions={0}, use_global_device_ids=true | all-gather | bytes 148992 | tf_op jit(solution)/shard_map/all_gather | solution.py:44
  74.8 9.3 %all-gather.4 = bf16[4,194,128]{2,1,0:T(8,128)(2,1)S(1)} all-gather(bf16[1,194,128]{2,1,0:T(8,128)(2,1)S(1)} %maximum_bitcast_fusion.1), channel_id=3, replica_groups=mesh['sp_0'=8,'sp_1'=4,'sp_2'=2,'tp'=4] {'sp_1'}, dimensions={0}, use_global_device_ids=true | all-gather | bytes 248320 | tf_op jit(solution)/shard_map/all_gather | solution.py:44
  87.2 0.6 fusion.271
  89.2 21.5 %all-gather.5 = bf16[8,194,128]{2,1,0:T(8,128)(2,1)S(1)} all-gather(bf16[1,194,128]{2,1,0:T(8,128)(2,1)S(1)} %maximum_bitcast_fusion.2), channel_id=4, replica_groups=mesh['sp_0'=8,'sp_1'=4,'sp_2'=2,'tp'=4] {'sp_0'}, dimensions={0}, use_global_device_ids=true | all-gather | bytes 446976 | tf_op jit(solution)/shard_map/all_gather | solution.py:44
  110.7 0.6 bitcast_convert_fusion.8
  111.9 0.6 slice_convert_fusion.11
  112.5 0.7 fusion.269
  113.8 0.7 copy.176
  114.5 0.7 copy.177
  115.3 0.7 copy.178
  116.1 0.7 copy.179
  116.9 0.7 copy.180
  117.6 0.8 reshape.1118
  118.4 0.7 copy.181
  119.1 0.8 reshape.1119
  119.9 0.7 copy.182
  120.6 0.8 reshape.1120
  121.5 0.7 copy.183
  122.2 0.8 reshape.1121
  123.0 0.7 copy.184
  123.8 0.7 copy.185
  124.6 0.7 copy.186
  125.4 1.6 fusion.292
  127.1 1.1 copy.170
  128.2 0.6 fusion.288
  134.7 1.2 copy.169
  136.6 1.2 fusion.291
  137.8 1.1 copy.153
  139.1 1.0 fusion.93
  140.1 2.7 add_convert_fusion
  142.8 4.8 %all-to-all-start = ((bf16[4,192,2048]{2,1,0:T(8,128)(2,1)}), bf16[4,192,2048]{2,1,0:T(8,128)(2,1)}, u32[]{:S(2)}, u32[]{:S(2)}) async-start(bf16[4,192,2048]{2,1,0:T(8,128)(2,1)} %bitcast.454), calls=%async_computation | async-start | bytes 6291456 | tf_op jit(solution)/shard_map/all_to_all | solution.py:84
  147.8 27.9 %all-to-all-done = bf16[4,192,2048]{2,1,0:T(8,128)(2,1)} async-done(((bf16[4,192,2048]{2,1,0:T(8,128)(2,1)}), bf16[4,192,2048]{2,1,0:T(8,128)(2,1)}, u32[]{:S(2)}, u32[]{:S(2)}) %all-to-all-start) | async-done | bytes 3145760 | tf_op jit(solution)/shard_map/all_to_all | solution.py:84
  175.8 2.7 convert_reduce_fusion
  178.8 1.1 fusion.63
  180.1 0.7 pad_maximum_fusion.2
  180.9 47.7 %all-gather.9.cloned.1.call-done = bf16[768,2048]{1,0:T(8,128)(2,1)} async-done(((bf16[192,2048]{1,0:T(8,128)(2,1)}), bf16[768,2048]{1,0:T(8,128)(2,1)}) %all-gather.9.cloned.1.call-update) | async-done | bytes 3145744 | tf_op jit(solution)/shard_map/all_gather | solution.py:225
  228.6 102.9 %all-gather.11.cloned.1.call-done = bf16[2048,4096]{1,0:T(8,128)(2,1)} async-done(((bf16[32,4096]{1,0:T(8,128)(2,1)}), bf16[2048,4096]{1,0:T(8,128)(2,1)}) %all-gather.11.cloned.1.call-update) | async-done | bytes 16777232 | tf_op jit(solution)/shard_map/all_gather | solution.py:22
  331.5 20.7 %fusion.55 = bf16[768,2048]{1,0:T(8,128)(2,1)} fusion(bf16[2048,4096]{1,0:T(8,128)(2,1)} %all-gather.11.cloned.1.call-done, bf16[768,2048]{1,0:T(8,128)(2,1)} %all-gather.9.cloned.1.call-done), kind=kOutput, calls=%fused_computation.75 | convolution fusion | flops 12891193344 | bytes 23068672 | tf_op jit(solution)/shard_map/dot_general | solution.py:228
  352.2 37.5 %reduce-scatter.2.cloned.1.call-done = bf16[192,2048]{1,0:T(8,128)(2,1)} async-done(((bf16[768,2048]{1,0:T(8,128)(2,1)}), bf16[192,2048]{1,0:T(8,128)(2,1)}) %reduce-scatter.2.cloned.1.call-update) | async-done | bytes 786448 | tf_op jit(solution)/shard_map/reduce_scatter | solution.py:229
  389.7 2.3 fusion.64
  (288 shorter events, 29.7 us)
Async XLA Ops:
  6.5 132.5 %copy-start = (bf16[128,2048]{1,0:T(8,128)(2,1)S(1)}, bf16[128,2048]{1,0:T(8,128)(2,1)}, u32[]{:S(2)}) copy-start(bf16[128,2048]{1,0:T(8,128)(2,1)} %param.31) | copy-start | bytes 1572868
  6.5 3.0 copy-start.6
  7.8 2.3 copy-start.9
  10.4 26.1 %copy-start.4 = (bf16[768,128]{1,0:T(8,128)(2,1)S(1)}, bf16[768,128]{1,0:T(8,128)(2,1)}, u32[]{:S(2)}) copy-start(bf16[768,128]{1,0:T(8,128)(2,1)} %param.21) | copy-start | bytes 589828
  10.4 26.0 %copy-start.5 = (bf16[768,128]{1,0:T(8,128)(2,1)S(1)}, bf16[768,128]{1,0:T(8,128)(2,1)}, u32[]{:S(2)}) copy-start(bf16[768,128]{1,0:T(8,128)(2,1)} %param.22) | copy-start | bytes 589828
  36.5 3.0 copy-start.14
  71.8 15.4 %copy-start.15 = (f32[2]{0:T(128)}, f32[2]{0:T(128)S(1)}, u32[]{:S(2)}) copy-start(f32[2]{0:T(128)S(1)} %bitcast_convert_fusion.12) | copy-start | bytes 28
  73.3 52.0 %copy-start.3 = (f32[6,128,2,64]{1,0,3,2:T(8,128)S(1)}, f32[6,128,2,64]{1,0,3,2:T(8,128)}, u32[]{:S(2)}) copy-start(f32[6,128,2,64]{1,0,3,2:T(8,128)} %get-tuple-element.84) | copy-start | bytes 1179652
  87.2 0.9 copy-start.12
  87.2 1.1 copy-start.11
  87.2 23.5 %copy-start.10 = (f32[2]{0:T(128)}, f32[2]{0:T(128)S(1)}, u32[]{:S(2)}) copy-start(f32[2]{0:T(128)S(1)} %get-tuple-element.255) | copy-start | bytes 28
  139.0 1.1 copy-start.2
  142.8 5.0 %copy-start.13 = (bf16[2048]{0:T(1024)(128)(2,1)S(1)}, bf16[2048]{0:T(1024)(128)(2,1)}, u32[]{:S(2)}) copy-start(bf16[2048]{0:T(1024)(128)(2,1)} %param.33) | copy-start | bytes 12292
  142.8 33.0 %all-to-all-start = ((bf16[4,192,2048]{2,1,0:T(8,128)(2,1)}), bf16[4,192,2048]{2,1,0:T(8,128)(2,1)}, u32[]{:S(2)}, u32[]{:S(2)}) async-start(bf16[4,192,2048]{2,1,0:T(8,128)(2,1)} %bitcast.454), calls=%async_computation | async-start | bytes 6291456 | tf_op jit(solution)/shard_map/all_to_all | solution.py:84
  147.6 30.9 %copy-start.1 = (bf16[192,2048]{1,0:T(8,128)(2,1)S(1)}, bf16[192,2048]{1,0:T(8,128)(2,1)}, u32[]{:S(2)}) copy-start(bf16[192,2048]{1,0:T(8,128)(2,1)} %param.20) | copy-start | bytes 2359300
  147.6 81.0 %all-gather.9.cloned.1.call-start = ((), (), s32[]{:S(2)}) async-start(), calls=%async_computation.2 | async-start | bytes 3932160 | tf_op jit(solution)/shard_map/all_gather | solution.py:225
  178.5 1.6 copy-start.7
  178.5 1.6 copy-start.8
  180.0 151.5 %all-gather.11.cloned.1.call-start = ((), (), s32[]{:S(2)}) async-start(), calls=%async_computation.3 | async-start | bytes 17039360 | tf_op jit(solution)/shard_map/all_gather | solution.py:22
  180.8 208.9 %reduce-scatter.2.cloned.1.call-start = ((), (), s32[]{:S(2)}) async-start(), calls=%async_computation.4 | async-start | bytes 3932160 | tf_op jit(solution)/shard_map/reduce_scatter | solution.py:229
Sparse Core Ops, SparseCore 0:
  180.1 48.4 all-gather.8
  231.4 100.0 all-gather.10
  352.4 37.3 reduce-scatter.1
where the time goes:
time: 400 us; the launch traced here: 399 us
  waiting for transfers between devices  216 us (54%)
  local copies, waits for them, and re-layouts  50.2 us (13%)
  matrix products  35.7 us (9%)
  blocking collectives  35.5 us (9%)
  between operations  26.9 us (7%)
  other arithmetic  24.5 us (6%)
  starting transfers between devices  5.08 us (1%)
  loops' own time  4.6 us (1%)
    all_gather x1, waiting for transfers between devices, rows_first(): out, at, finished = (lax.all_gather(both, axis, axis=0, tiled=True), 0, [])  103 us
    all_gather x1, waiting for transfers between devices, on_device(): lax.all_gather(row_norm(middle, norm_gain), 'tp', axis=0, tiled=True)  47.7 us
    reduce_scatter x1, waiting for transfers between devices, on_device(): lax.psum_scatter(down_sum.astype(jnp.bfloat16), 'tp', scatter_dimension=0...  37.5 us
    all_gather x3, blocking collectives, gathered_once(): both, at, found = (lax.all_gather(jnp.concatenate(lines), axis), 0, {})  35.5 us
    all_to_all x1, waiting for transfers between devices, sum_at_owner(): lax.all_to_all(tiles, axis, split_axis=0, concat_axis=0, tiled=True)  27.9 us
    dynamic_update_slice x18, local copies, waits for them, and re-layouts, local_group(): lax.scan(block_step, carried, (query_rot.reshape(blocks, BLOCK, count_of_...  21.1 us
    dot_general x1, matrix products, on_device(): down_sum = jnp.dot(hidden, down_full, preferred_element_type=jnp.float32)  20.7 us
    convert_element_type x28, local copies, waits for them, and re-layouts, entering(): part[k].astype(own.dtype)  12.1 us
  transfers between devices with their start and end apart: 4, of which 4 were waited for; matrix products, arithmetic and copies ran while one was open for 0% of the time, Pallas kernels for 0%

commit v1 on v0

v1 whole, which is shorter than its diff:
```python
import functools

import jax
import jax.numpy as jnp
import numpy as np
from jax import lax
from jax.experimental import pallas as pl
from jax.experimental.pallas import tpu as pltpu
from jax.sharding import Mesh
from jax.sharding import PartitionSpec as P

HDW = 128
HDN = 64
BLOCK = 128
head_eps = 1e-05
norm_eps = 1e-06
rope_base = 10000.0
MESH = pl.DeviceIdType.MESH
F32 = jnp.float32
BF16 = jnp.bfloat16


def rope_tables(steps, stride):
    tables = []
    for width in (HDW, HDN):
        half = width // 2
        inverse = rope_base ** (-np.arange(half, dtype=np.float64) / half)
        lanes = np.tile(inverse, 128 // half)
        angles = (stride * np.arange(steps, dtype=np.float64))[:, None] * lanes[None, :]
        tables += [np.cos(angles), np.sin(angles)]
    return np.stack(tables).astype(np.float32)


def remote(src, dst, send_sem, recv_sem, device):
    return pltpu.make_async_remote_copy(
        src_ref=src, dst_ref=dst, send_sem=send_sem, recv_sem=recv_sem, device_id=device, device_id_type=MESH
    )


def turn(cos_a, sin_a, cos_b, sin_b):
    return cos_a * cos_b - sin_a * sin_b, sin_a * cos_b + cos_a * sin_b


def dot(a, b):
    return jnp.dot(a, b, preferred_element_type=F32)


def dot_t(a, b):
    return lax.dot_general(a, b, (((1,), (1,)), ((), ())), preferred_element_type=F32)


def tdot(a, b):
    return lax.dot_general(a, b, (((0,), (0,)), ((), ())), preferred_element_type=F32)


def kernel(
    sizes,
    stream, qw, kw, vw, gw, dw, qn, kn, vn, gn, dn, gain, tt, tb, ts, wo, up, down,
    out,
    stream_all, qe_w, qe_n, o_w, o_n, decays, msg, in1, pre1, tot2, in2, msg3, in3,
    mixed, middle, normed, hidden, send2, send1, sendm, own, relay_l, relay_r, got_l, got_r,
    st_s, st_r, s1_s, s1_r, s2_s, s2_r, s3_s, s3_r, mx_s, mx_r, rs_s, rs_r,
):
    nz, ny, nc, nx = sizes
    z, y, c, x = (lax.axis_index(a) for a in ("z", "y", "c", "x"))
    xr, xl, xo = lax.rem(x + 1, nx), lax.rem(x + nx - 1, nx), lax.rem(x + 2, nx)
    plane = ny * nc
    me = y * nc + c
    sp = z * plane + me
    tok = qw.shape[0]
    blocks = tok // BLOCK
    rows = stream.shape[0]
    half_rows = rows // 2
    right, left = {"x": xr}, {"x": xl}

    def at_plane(j):
        return {"y": j // nc, "c": lax.rem(j, nc)}

    barrier = pltpu.get_barrier_semaphore()
    peers = [right, left]
    peers += [at_plane(lax.rem(me + d, plane)) for d in range(1, plane)]
    peers += [{"z": lax.rem(z + d, nz)} for d in range(1, nz)]
    for peer in peers:
        pl.semaphore_signal(barrier, inc=1, device_id=peer, device_id_type=MESH)
    pl.semaphore_wait(barrier, len(peers))

    to_r = remote(stream, stream_all.at[x], st_s.at[0], st_r.at[0], right)
    to_l = remote(stream, stream_all.at[x], st_s.at[1], st_r.at[1], left)
    to_r.start()
    to_l.start()
    stream_all[pl.ds(x, 1)] = stream[...][None]

    lane = lax.broadcasted_iota(jnp.int32, (1, 128), 1)
    low = lane < HDN
    base = []
    for g in (0, 2):
        row = [ts[g + i, pl.ds(sp, 1), :] for i in (0, 1)]
        base.append(turn(row[0], row[1], tb[g], tb[g + 1]))
    sign_w = jnp.where(lane < HDW // 2, -1.0, 1.0)
    front_n = lax.rem(lane, HDN) < HDN // 2
    sign_n = jnp.where(front_n, -1.0, 1.0)

    decays[...] = jnp.zeros_like(decays)
    for b in range(blocks):
        cut = pl.ds(b * BLOCK, BLOCK)
        decays[pl.ds(3 * b, 1), :] = dw[:, cut]
        decays[pl.ds(3 * b + 1, 2), :] = dn[:, cut]
    running = decays[0:32, :]
    shift = 1
    while shift < BLOCK:
        running = running + jnp.where(lane >= shift, pltpu.roll(running, shift, 1), 0.0)
        shift *= 2
    decays[0:32, :] = running
    columns = jnp.transpose(decays[...])

    at_t = lax.broadcasted_iota(jnp.int32, (BLOCK, BLOCK), 0)
    at_s = lax.broadcasted_iota(jnp.int32, (BLOCK, BLOCK), 1)
    lower = at_t >= at_s
    same_head = (at_t < HDN) == (at_s < HDN)

    def spread(r):
        steps = jnp.minimum(columns[:, r : r + 1] - decays[pl.ds(r, 1), :], 0.0)
        return jnp.where(lower, jnp.exp(steps), 0.0)

    state_w = jnp.zeros((128, 128), F32)
    state_n = jnp.zeros((128, 128), F32)
    gone = [jnp.zeros((1, 1), F32)] * 3
    for b in range(blocks):
        cut = pl.ds(b * BLOCK, BLOCK)
        r = 3 * b
        now = [columns[:, r + h : r + h + 1] for h in range(3)]
        last = [columns[BLOCK - 1 : BLOCK, r + h : r + h + 1] for h in range(3)]
        cos, sin = turn(base[0][0][b : b + 1], base[0][1][b : b + 1], tt[0], tt[1])
        sin = sin * sign_w
        q = qw[cut, :].astype(F32)
        k = kw[cut, :].astype(F32)
        v = vw[cut, :]
        q = q * cos + pltpu.roll(q, HDW // 2, 1) * sin
        k = (k * cos + pltpu.roll(k, HDW // 2, 1) * sin) * HDW**-0.5
        scores = dot_t(q.astype(BF16), k.astype(BF16)) * spread(r)
        out_b = dot(scores.astype(BF16), v)
        if b:
            out_b += dot((q * jnp.exp(now[0])).astype(BF16), state_w.astype(BF16))
        o_w[cut, :] = out_b
        qe_w[cut, :] = (q * jnp.exp(now[0] + gone[0])).astype(BF16)
        tail = k * jnp.exp(last[0] - now[0])
        state_w = jnp.exp(last[0]) * state_w + tdot(tail.astype(BF16), v)
        cos, sin = turn(base[1][0][b : b + 1], base[1][1][b : b + 1], tt[2], tt[3])
        sin = sin * sign_n
        q = qn[cut, :].astype(F32)
        k = kn[cut, :].astype(F32)
        v = vn[cut, :]

        def other(a):
            return jnp.where(front_n, pltpu.roll(a, 128 - HDN // 2, 1), pltpu.roll(a, HDN // 2, 1))

        q = q * cos + other(q) * sin
        k = (k * cos + other(k) * sin) * HDN**-0.5
        kb = k.astype(BF16)
        probs = []
        for h, mask in enumerate((low, jnp.logical_not(low))):
            qh = jnp.where(mask, q, 0.0).astype(BF16)
            probs.append((dot_t(qh, kb) * spread(r + 1 + h)).astype(BF16))
        v_f = v.astype(F32)
        v2 = jnp.concatenate(
            [jnp.where(low, v_f, 0.0).astype(BF16), jnp.where(low, 0.0, v_f).astype(BF16)], axis=0
        )
        out_b = dot(jnp.concatenate(probs, axis=1), v2)
        if b:
            seen = jnp.where(low, jnp.exp(now[1]), jnp.exp(now[2]))
            out_b += dot((q * seen).astype(BF16), state_n.astype(BF16))
        o_n[cut, :] = out_b
        seen = jnp.where(low, jnp.exp(now[1] + gone[1]), jnp.exp(now[2] + gone[2]))
        qe_n[cut, :] = (q * seen).astype(BF16)
        tail = k * jnp.where(low, jnp.exp(last[1] - now[1]), jnp.exp(last[2] - now[2]))
        keep = jnp.where(low, jnp.exp(last[1]), jnp.exp(last[2]))
        state_n = keep * state_n + jnp.where(same_head, tdot(tail.astype(BF16), v), 0.0)
        gone = [g + t for g, t in zip(gone, last)]

    total_w = jnp.exp(gone[0]) + jnp.zeros((1, 128), F32)
    total_n = jnp.where(low, jnp.exp(gone[1]), jnp.exp(gone[2]))
    packed_n = jnp.where(low, state_n[:HDN], state_n[HDN:])
    sw, sn = 128 // plane, HDN // plane
    for j in range(plane):
        msg[j, 0:sw, :] = state_w[sw * j : sw * (j + 1)]
        msg[j, sw : sw + sn, :] = packed_n[sn * j : sn * (j + 1)]
        msg[j, sw + sn : sw + sn + 1, :] = total_w
        msg[j, sw + sn + 1 : sw + sn + 2, :] = total_n
    ns = sw + sn

    def stage1(d):
        to = lax.rem(me + d, plane)
        return remote(msg.at[to], in1.at[me], s1_s.at[d], s1_r.at[d], at_plane(to))

    for d in range(1, plane):
        stage1(d).start()
    in1[pl.ds(me, 1)] = msg[pl.ds(me, 1)]

    to_r.wait_recv()
    on_r = remote(
        stream_all.at[xl, pl.ds(0, half_rows)], stream_all.at[xl, pl.ds(0, half_rows)],
        st_s.at[2], st_r.at[2], right,
    )
    on_r.start()
    to_l.wait_recv()
    on_l = remote(
        stream_all.at[xr, pl.ds(half_rows, half_rows)], stream_all.at[xr, pl.ds(half_rows, half_rows)],
        st_s.at[3], st_r.at[3], left,
    )
    on_l.start()

    for d in range(1, plane):
        stage1(d).wait_recv()
    wide_row = lax.broadcasted_iota(jnp.int32, (ns, 128), 0) < sw

    def factor(pair):
        return jnp.where(wide_row, pair[0], pair[1])

    def rates(ref, j):
        return ref[j, ns : ns + 1, :], ref[j, ns + 1 : ns + 2, :]

    held = jnp.zeros((ns, 128), F32)
    rate = (jnp.ones((1, 128), F32), jnp.ones((1, 128), F32))
    for j in range(plane):
        pre1[j, 0:ns, :] = held
        pre1[j, ns : ns + 1, :] = rate[0]
        pre1[j, ns + 1 : ns + 2, :] = rate[1]
        mine = rates(in1, j)
        held = held * factor(mine) + in1[j, 0:ns, :]
        rate = (rate[0] * mine[0], rate[1] * mine[1])
    tot2[0:ns, :] = held
    tot2[ns : ns + 1, :] = rate[0]
    tot2[ns + 1 : ns + 2, :] = rate[1]

    def stage2(d):
        return remote(tot2, in2.at[z], s2_s.at[d], s2_r.at[d], {"z": lax.rem(z + d, nz)})

    for d in range(1, nz):
        stage2(d).start()
    in2[pl.ds(z, 1)] = tot2[...][None]
    for d in range(1, nz):
        stage2(d).wait_recv()
    held = jnp.zeros((ns, 128), F32)
    for k in range(nz):
        later = held * factor(rates(in2, k)) + in2[k, 0:ns, :]
        held = jnp.where(k < z, later, held)
    for j in range(plane):
        msg3[j] = held * factor(rates(pre1, j)) + pre1[j, 0:ns, :]

    def stage3(d):
        to = lax.rem(me + d, plane)
        return remote(msg3.at[to], in3.at[me], s3_s.at[d], s3_r.at[d], at_plane(to))

    for d in range(1, plane):
        stage3(d).start()
    in3[pl.ds(me, 1)] = msg3[pl.ds(me, 1)]
    for d in range(1, plane):
        stage3(d).wait_recv()
    arrived = in3[...]
    enter_w = arrived[:, 0:sw, :].reshape(128, 128).astype(BF16)
    enter_p = arrived[:, sw:ns, :].reshape(HDN, 128)
    enter_n = jnp.concatenate(
        [jnp.where(low, enter_p, 0.0), jnp.where(low, 0.0, enter_p)], axis=0
    ).astype(BF16)

    def mixed_to(i, side):
        return remote(
            mixed.at[x, i], mixed.at[x, i], mx_s.at[side, i], mx_r.at[side, i], (right, left)[side]
        )

    def gated(o, gate):
        return (o * jax.nn.silu(gate.astype(F32))).astype(BF16)

    for i in range(nx):
        cut = pl.ds(i * rows, rows)
        o = o_w[cut, :] + dot(qe_w[cut, :], enter_w)
        o = o - jnp.mean(o, axis=-1, keepdims=True)
        o = o * lax.rsqrt(jnp.mean(o * o, axis=-1, keepdims=True) + head_eps)
        mixed[x, i, :, 0:128] = gated(o, gw[cut, :])
        o = o_n[cut, :] + dot(qe_n[cut, :], enter_n)

        def by_head(a):
            first = jnp.sum(jnp.where(low, a, 0.0), axis=-1, keepdims=True)
            second = jnp.sum(jnp.where(low, 0.0, a), axis=-1, keepdims=True)
            return jnp.where(low, first, second) * (1.0 / HDN)

        o = o - by_head(o)
        o = o * lax.rsqrt(by_head(o * o) + head_eps)
        mixed[x, i, :, 128:256] = gated(o, gn[cut, :])
        mixed_to(i, 0).start()
        mixed_to(i, 1).start()

    def mixed_on(i, side):
        src, start = ((xl, 0), (xr, half_rows))[side]
        piece = mixed.at[src, i, pl.ds(start, half_rows)]
        return remote(piece, piece, mx_s.at[2 + side, i], mx_r.at[2 + side, i], (right, left)[side])

    def pass_on(i, _):
        for side in (0, 1):
            mixed_to(i, side).wait_recv()
            mixed_on(i, side).start()
        return 0

    lax.fori_loop(0, nx, pass_on, 0)
    on_r.wait_recv()
    on_l.wait_recv()

    width = stream.shape[1]
    tile = 512
    tiles = width // tile

    def rows_in(i, _):
        mixed_on(i, 0).wait_recv()
        mixed_on(i, 1).wait_recv()

        def project(n, squares):
            at = pl.ds(pl.multiple_of(n * tile, tile), tile)
            total = stream_all[i, :, at].astype(F32)
            for j in range(nx):
                total += dot(mixed[j, i], wo[j, :, at])
            total = total.astype(BF16)
            middle[i, :, at] = total
            total = total.astype(F32)
            return squares + jnp.sum(total * total, axis=-1, keepdims=True)

        squares = lax.fori_loop(0, tiles, project, jnp.zeros((rows, 1), F32))
        scale = lax.rsqrt(squares * (1.0 / width) + norm_eps)
        normed[...] = (middle[i].astype(F32) * scale * gain[...].astype(F32)).astype(BF16)

        def rise(n, _):
            at = pl.ds(pl.multiple_of(n * tile, tile), tile)
            h = jnp.maximum(dot(normed[...], up[:, at]), 0.0)
            hidden[i, :, at] = (h * h).astype(BF16)
            return 0

        lax.fori_loop(0, tiles, rise, 0)
        return 0

    lax.fori_loop(0, nx, rows_in, 0)

    side_tiles = tiles // 2

    def fall(i, side, into):
        def one(n, _):
            at = pl.ds(pl.multiple_of(n * tile, tile), tile)
            part = dot_t(hidden[i], down[pl.ds(pl.multiple_of((side * side_tiles + n) * tile, tile), tile), :])
            into[side, :, at] = part.astype(into.dtype)
            return 0

        lax.fori_loop(0, side_tiles, one, 0)

    far = [
        remote(send2.at[0], relay_l, rs_s.at[0], rs_r.at[0], right),
        remote(send2.at[1], relay_r, rs_s.at[1], rs_r.at[1], left),
    ]
    near_r = [remote(send1.at[s], got_l.at[s], rs_s.at[2 + s], rs_r.at[2 + s], right) for s in (0, 1)]
    near_l = [remote(sendm.at[s], got_r.at[s], rs_s.at[4 + s], rs_r.at[4 + s], left) for s in (0, 1)]
    fall(xo, 0, send2)
    far[0].start()
    fall(xo, 1, send2)
    far[1].start()
    fall(xr, 1, send1)
    near_r[1].start()
    fall(xl, 0, sendm)
    near_l[0].start()
    fall(xr, 0, own)
    fall(xl, 1, own)
    far[0].wait_recv()
    send1[0] = (own[0] + relay_l[...].astype(F32)).astype(BF16)
    near_r[0].start()
    far[1].wait_recv()
    sendm[1] = (own[1] + relay_r[...].astype(F32)).astype(BF16)
    near_l[1].start()
    fall(x, 0, own)
    fall(x, 1, own)
    span = width // 2
    for s, first, second in ((1, near_r, near_l), (0, near_l, near_r)):
        first[s].wait_recv()
        second[s].wait_recv()
        at = slice(s * span, (s + 1) * span)
        total = own[s] + got_l[s].astype(F32) + got_r[s].astype(F32)
        out[:, at] = (middle[x, :, at].astype(F32) + total).astype(BF16)

    for copy in (to_r, to_l, on_r, on_l, *far, *near_r, *near_l):
        copy.wait_send()
    for d in range(1, plane):
        stage1(d).wait_send()
        stage3(d).wait_send()
    for d in range(1, nz):
        stage2(d).wait_send()
    for i in range(nx):
        for side in (0, 1):
            mixed_to(i, side).wait_send()
            mixed_on(i, side).wait_send()


def on_device(
    sizes,
    stream_in, query_wide, key_wide, value_wide, gate_wide, decay_wide,
    query_narrow, key_narrow, value_narrow, gate_narrow, decay_narrow,
    output_wide, output_narrow, norm_gain, up_weight, down_weight,
):
    nz, ny, nc, nx = sizes
    tok = query_wide.shape[0]
    rows, width = stream_in.shape
    plane = ny * nc
    sp_axes = ("z", "y", "c")
    both = jnp.concatenate([up_weight, down_weight.T], axis=1)
    both = lax.all_gather(both, sp_axes, axis=0, tiled=True)
    hid = up_weight.shape[1]
    up, down = both[:, :hid], both[:, hid:]
    wo = lax.all_gather(jnp.concatenate([output_wide, output_narrow], axis=0), "x")
    ns = (128 + HDN) // plane
    dma = pltpu.SemaphoreType.DMA
    vm = pltpu.VMEM
    scratch = [
        vm((nx, rows, width), BF16),
        vm((tok, 128), BF16), vm((tok, 128), BF16), vm((tok, 128), F32), vm((tok, 128), F32),
        vm((128, 128), F32),
        vm((plane, ns + 8, 128), F32), vm((plane, ns + 8, 128), F32), vm((plane, ns + 8, 128), F32),
        vm((ns + 8, 128), F32), vm((nz, ns + 8, 128), F32),
        vm((plane, ns, 128), F32), vm((plane, ns, 128), F32),
        vm((nx, nx, rows, 256), BF16),
        vm((nx, rows, width), BF16), vm((rows, width), BF16), vm((nx, rows, hid), BF16),
        vm((2, rows, width // 2), BF16), vm((2, rows, width // 2), BF16), vm((2, rows, width // 2), BF16),
        vm((2, rows, width // 2), F32),
        vm((rows, width // 2), BF16), vm((rows, width // 2), BF16),
        vm((2, rows, width // 2), BF16), vm((2, rows, width // 2), BF16),
        dma((4,)), dma((4,)),
        dma((plane,)), dma((plane,)), dma((nz,)), dma((nz,)), dma((plane,)), dma((plane,)),
        dma((4, nx)), dma((4, nx)), dma((6,)), dma((6,)),
    ]
    vmem = pl.BlockSpec(memory_space=pltpu.VMEM)
    return pl.pallas_call(
        functools.partial(kernel, sizes),
        out_shape=jax.ShapeDtypeStruct((rows, width), BF16),
        in_specs=[vmem] * 18,
        out_specs=vmem,
        scratch_shapes=scratch,
        compiler_params=pltpu.CompilerParams(
            collective_id=0, has_side_effects=True, vmem_limit_bytes=60 * 1024 * 1024
        ),
    )(
        stream_in, query_wide, key_wide, value_wide, gate_wide, decay_wide,
        query_narrow, key_narrow, value_narrow, gate_narrow, decay_narrow,
        norm_gain[None], jnp.asarray(rope_tables(BLOCK, 1)), jnp.asarray(rope_tables(8, BLOCK)),
        jnp.asarray(rope_tables(nz * plane, tok)), wo, up, down,
    )


def solution(mesh):
    sizes = (8, 4, 2, mesh.shape["tp"])
    split = Mesh(mesh.devices.reshape(sizes), ("z", "y", "c", "x"))
    sp = ("z", "y", "c")
    rows, heads = P(sp, "x"), P("x", sp)
    in_specs = (
        P((*sp, "x"), None), rows, rows, rows, rows, heads, rows, rows, rows, rows, heads,
        P("x", None), P("x", None), P(), rows, heads,
    )
    return jax.shard_map(
        functools.partial(on_device, sizes), mesh=split, in_specs=in_specs,
        out_specs=P((*sp, "x"), None), check_vma=False,
    )
```

time: 400 us -> 276 us (0.69)
  Pallas kernels: 0 us -> 103 us
  waiting for transfers between devices: 216 us -> 139 us
  matrix products: 35.7 us -> 0 us
  blocking collectives: 35.5 us -> 0 us
  local copies, waits for them, and re-layouts: 50.2 us -> 15.4 us
  other arithmetic: 24.5 us -> 3.98 us
  between operations: 26.9 us -> 13.4 us
  starting transfers between devices: 5.08 us -> 0.04 us
  loops' own time: 4.6 us -> 0 us
    pallas_call x0 -> x1, Pallas kernels: none -> 103 us  [on_device(): pl.pallas_call(functools.partial(kernel, sizes), out_shape=jax.ShapeDtype...]
    reduce_scatter x1 -> x0, waiting for transfers between devices: 37.5 us -> none  [on_device(): lax.psum_scatter(down_sum.astype(jnp.bfloat16), 'tp', scatter_dimension=0...]
    dot_general x41 -> x0, matrix products: 35.7 us -> none  [the longest x1 20.7 us: on_device(): down_sum = jnp.dot(hidden, down_full, preferred_element_type=jnp.float32)]
    all_gather x3 -> x0, blocking collectives: 35.5 us -> none  [gathered_once(): both, at, found = (lax.all_gather(jnp.concatenate(lines), axis), 0, {})]
    all_to_all x1 -> x0, waiting for transfers between devices: 27.9 us -> none  [sum_at_owner(): lax.all_to_all(tiles, axis, split_axis=0, concat_axis=0, tiled=True)]
    dynamic_update_slice x18 -> x0, local copies, waits for them, and re-layouts: 21.1 us -> none  [local_group(): lax.scan(block_step, carried, (query_rot.reshape(blocks, BLOCK, count_of_...]
    convert_element_type x28 -> x0, local copies, waits for them, and re-layouts: 12.1 us -> none  [entering(): part[k].astype(own.dtype)]
    all_gather x2, waiting for transfers between devices: 151 us -> 139 us  [the longest x1 102 us: on_device(): both = lax.all_gather(both, sp_axes, axis=0, tiled=True)]
  transfers between devices with their start and end apart: 4 -> 2, of which waited for: 4 -> 2; matrix products, arithmetic and copies ran while one was open for 0% -> 6% of each run, Pallas kernels for 0% -> 0%
where the time goes in v1:
time: 276 us; the launch traced here: 274 us
  waiting for transfers between devices  139 us (50%)
  Pallas kernels  103 us (37%)
  local copies, waits for them, and re-layouts  15.4 us (6%)
  between operations  13.4 us (5%)
  other arithmetic  3.98 us (1%)
    pallas_call x1, Pallas kernels, on_device(): pl.pallas_call(functools.partial(kernel, sizes), out_shape=jax.ShapeDtype...  103 us
    all_gather x1, waiting for transfers between devices, on_device(): both = lax.all_gather(both, sp_axes, axis=0, tiled=True)  102 us
    all_gather x1, waiting for transfers between devices, on_device(): lax.all_gather(jnp.concatenate([output_wide, output_narrow], axis=0), 'x')  37 us
    slice x1, local copies, waits for them, and re-layouts, on_device(): up, down = (both[:, :hid], both[:, hid:])  12 us
  transfers between devices with their start and end apart: 2, of which 2 were waited for; matrix products, arithmetic and copies ran while one was open for 6% of the time, Pallas kernels for 0%

profile of v1, /device:TPU:1, one launch (start us, length us, event | category | flops | bytes accessed | tf_op | source)
XLA Modules:
  0.0 274.5 jit_solution(15116824070650153607)
XLA Ops:
  6.5 0.0 all-gather.4.cloned.1.call-start
  6.5 1.7 pad_maximum_fusion.1
  8.2 0.0 all-gather.4.cloned.1.call-update
  8.2 0.0 all-gather.6.cloned.1.call-start
  8.3 2.3 pad_maximum_fusion
  10.6 0.0 all-gather.6.cloned.1.call-update
  10.6 1.3 broadcast_in_dim.3.gain
  11.9 101.7 %all-gather.4.cloned.1.call-done = bf16[2048,4096]{1,0:T(8,128)(2,1)} async-done(((bf16[32,4096]{1,0:T(8,128)(2,1)}), bf16[2048,4096]{1,0:T(8,128)(2,1)}) %all-gather.4.cloned.1.call-update) | async-done | bytes 16777232 | tf_op jit(solution)/shard_map/all_gather | solution.py:409
  113.6 12.0 %fusion = (bf16[2048,2048]{1,0:T(8,128)(2,1)}, bf16[2048,2048]{1,0:T(8,128)(2,1)}) fusion(bf16[2048,4096]{1,0:T(8,128)(2,1)} %all-gather.4.cloned.1.call-done), kind=kLoop, calls=%fused_computation.2 | loop fusion | bytes 33554432 | tf_op jit(solution)/shard_map/slice | solution.py:411
  125.6 37.0 %all-gather.6.cloned.1.call-done = bf16[1024,2048]{1,0:T(8,128)(2,1)} async-done(((bf16[256,2048]{1,0:T(8,128)(2,1)}), bf16[1024,2048]{1,0:T(8,128)(2,1)}) %all-gather.6.cloned.1.call-update) | async-done | bytes 4194320 | tf_op jit(solution)/shard_map/all_gather | solution.py:412
  162.6 103.0 %shard_map.181 = bf16[192,2048]{1,0:T(8,128)(2,1)} custom-call(bf16[192,2048]{1,0:T(8,128)(2,1)} %stream.1, bf16[768,128]{1,0:T(8,128)(2,1)} %qw.1, bf16[768,128]{1,0:T(8,128)(2,1)} %kw.1, bf16[768,128]{1,0:T(8,128)(2,1)} %vw.1, bf16[768,128]{1,0:T(8,128)(2,1)} %gw.1, f32[1,768]{1,0:T(1,128)} %dw.1, bf16[768,128]{1,0:T(8,128)(2,1)} %qn.1, ...), custom_call_target="tpu_custom_call" | custom-call | tf_op jit(solution)/shard_map/pallas_call | solution.py:434
  265.6 2.1 copy.21
Async XLA Ops:
  6.5 107.1 %all-gather.4.cloned.1.call-start = ((), (), s32[]{:S(2)}) async-start(), calls=%async_computation | async-start | bytes 17039360 | tf_op jit(solution)/shard_map/all_gather | solution.py:409
  8.2 154.3 %all-gather.6.cloned.1.call-start = ((), (), s32[]{:S(2)}) async-start(), calls=%async_computation.1 | async-start | bytes 5242880 | tf_op jit(solution)/shard_map/all_gather | solution.py:412
Sparse Core Ops, SparseCore 0:
  10.1 103.4 all-gather.3
  115.4 47.1 all-gather.5

commit v2 on v1

--- a/solution.py
+++ b/solution.py
@@ -55,11 +55,13 @@
 
 def kernel(
     sizes,
-    stream, qw, kw, vw, gw, dw, qn, kn, vn, gn, dn, gain, tt, tb, ts, wo, up, down,
+    stream, qw, kw, vw, gw, dw, qn, kn, vn, gn, dn, gain, tt, tb, ts, ow, on, up_own, down_own,
     out,
+    up, down, wo,
     stream_all, qe_w, qe_n, o_w, o_n, decays, msg, in1, pre1, tot2, in2, msg3, in3,
     mixed, middle, normed, hidden, send2, send1, sendm, own, relay_l, relay_r, got_l, got_r,
     st_s, st_r, s1_s, s1_r, s2_s, s2_r, s3_s, s3_r, mx_s, mx_r, rs_s, rs_r,
+    in_s, wo_s, wo_r, uz_s, uz_r, uy_s, uy_r, ur_s, ur_r, dy_s, dy_r, dz_s, dz_r, core_s, core_r,
 ):
     nz, ny, nc, nx = sizes
     z, y, c, x = (lax.axis_index(a) for a in ("z", "y", "c", "x"))
@@ -70,11 +72,22 @@
     tok = qw.shape[0]
     blocks = tok // BLOCK
     rows = stream.shape[0]
+    width = stream.shape[1]
     half_rows = rows // 2
     right, left = {"x": xr}, {"x": xl}
 
     def at_plane(j):
         return {"y": j // nc, "c": lax.rem(j, nc)}
+
+    loads = [
+        pltpu.make_async_copy(up_own, up.at[z, y, c], in_s.at[0]),
+        pltpu.make_async_copy(down_own, down.at[z, y, c], in_s.at[1]),
+        pltpu.make_async_copy(ow, wo.at[x, 0], in_s.at[2]),
+        pltpu.make_async_copy(on, wo.at[x, 1], in_s.at[3]),
+        pltpu.make_async_copy(stream, stream_all.at[x], in_s.at[4]),
+    ]
+    for load in loads:
+        load.start()
 
     barrier = pltpu.get_barrier_semaphore()
     peers = [right, left]
@@ -84,11 +97,225 @@
         pl.semaphore_signal(barrier, inc=1, device_id=peer, device_id_type=MESH)
     pl.semaphore_wait(barrier, len(peers))
 
-    to_r = remote(stream, stream_all.at[x], st_s.at[0], st_r.at[0], right)
-    to_l = remote(stream, stream_all.at[x], st_s.at[1], st_r.at[1], left)
+    sent = []
+
+    def go(copy):
+        copy.start()
+        sent.append(copy)
+
+    def same(ref, send_sem, recv_sem, device):
+        return remote(ref, ref, send_sem, recv_sem, device)
+
+    z_to = ({"z": lax.rem(z + 1, nz)}, {"z": lax.rem(z + nz - 1, nz)})
+    y_to = ({"y": lax.rem(y + 1, ny)}, {"y": lax.rem(y + ny - 1, ny)})
+    x_to = (right, left)
+    partner = {"c": 1 - c}
+    fwd = (1, -1)
+
+    def at_z(k):
+        return lax.rem(z + nz + k, nz)
+
+    def at_y(k):
+        return lax.rem(y + ny + k, ny)
+
+    def at_x(k):
+        return lax.rem(x + nx + k, nx)
+
+    part = up.shape[3]
+    halves = (pl.ds(0, part // 2), pl.ds(part // 2, part // 2))
+
+    def uz(step, side):
+        ref = up.at[at_z(-fwd[side] * (step - 1)), y, c]
+        if step == nz // 2:
+            ref = ref.at[halves[side]]
+        return same(ref, uz_s.at[side, step - 1], uz_r.at[side, step - 1], z_to[side])
+
+    def uz_in(step, side):
+        ref = up.at[at_z(-fwd[side] * step), y, c]
+        if step == nz // 2:
+            ref = ref.at[halves[side]]
+        return same(ref, uz_s.at[side, step - 1], uz_r.at[side, step - 1], z_to[side])
+
+    def uy(off, side):
+        return same(up.at[at_z(off), y, c], uy_s.at[side, off % nz], uy_r.at[side, off % nz], y_to[side])
+
+    def uy_in(off, side):
+        ref = up.at[at_z(off), at_y(-fwd[side]), c]
+        return same(ref, uy_s.at[side, off % nz], uy_r.at[side, off % nz], y_to[side])
+
+    relayed = ((0, 1, 2, 3), (4, -1, -2, -3))
+
+    def ur(i, side):
+        ref = up.at[at_z(relayed[side][i]), at_y(-fwd[side]), c]
+        return same(ref, ur_s.at[side, i], ur_r.at[side, i], y_to[side])
+
+    def ur_in(i, side):
+        ref = up.at[at_z(relayed[side][i]), at_y(2), c]
+        return same(ref, ur_s.at[side, i], ur_r.at[side, i], y_to[side])
+
+    def u_core(i):
+        ref = up.at[:, at_y((0, 1, -1, 2)[i]), c]
+        return same(ref, core_s.at[i], core_r.at[i], partner)
+
+    def u_core_in(i):
+        ref = up.at[:, at_y((0, 1, -1, 2)[i]), 1 - c]
+        return same(ref, core_s.at[i], core_r.at[i], partner)
+
+    def u_own():
+        for side in (0, 1):
+            go(uz(1, side))
+        for side in (0, 1):
+            go(uy(0, side))
+
+    def u_step(step):
+        for side in (0, 1):
+            uz_in(step, side).wait_recv()
+            if step < nz // 2:
+                go(uz(step + 1, side))
+        offs = (-step, step) if step < nz // 2 else (step,)
+        for off in offs:
+            for side in (0, 1):
+                go(uy(off, side))
+        if step == nz // 2:
+            go(u_core(0))
+
+    def u_relay(*which):
+        for i, side in which:
+            uy_in(relayed[side][i], side).wait_recv()
+            go(ur(i, side))
+
+    def u_rest():
+        for side in (0, 1):
+            for off in relayed[1 - side]:
+                uy_in(off, side).wait_recv()
+        go(u_core(1))
+        go(u_core(2))
+
+    def u_last():
+        for side in (0, 1):
+            for i in range(nz // 2):
+                ur_in(i, side).wait_recv()
+        go(u_core(3))
+
+    def u_done():
+        for i in range(ny):
+            u_core_in(i).wait_recv()
+
+    def dy(step, side):
+        ref = down.at[z, at_y(-fwd[side] * (step - 1)), c]
+        if step == 2:
+            ref = ref.at[halves[side]]
+        return same(ref, dy_s.at[side, step - 1], dy_r.at[side, step - 1], y_to[side])
+
+    def dy_in(step, side):
+        ref = down.at[z, at_y(-fwd[side] * step), c]
+        if step == 2:
+            ref = ref.at[halves[side]]
+        return same(ref, dy_s.at[side, step - 1], dy_r.at[side, step - 1], y_to[side])
+
+    columns_y = (0, 1, -1, 2)
+    last_by = ((0, 1), (2, 3))
+
+    def dz(step, side, g):
+        ref = down.at[at_z(-fwd[side] * (step - 1)), at_y(columns_y[g]), c]
+        return same(ref, dz_s.at[side, step - 1, g], dz_r.at[side, step - 1, g], z_to[side])
+
+    def dz_in(step, side, g):
+        ref = down.at[at_z(-fwd[side] * step), at_y(columns_y[g]), c]
+        return same(ref, dz_s.at[side, step - 1, g], dz_r.at[side, step - 1, g], z_to[side])
+
+    def d_core(k):
+        return same(down.at[at_z(k), :, c], core_s.at[4 + k % nz], core_r.at[4 + k % nz], partner)
+
+    def d_core_in(k):
+        return same(down.at[at_z(k), :, 1 - c], core_s.at[4 + k % nz], core_r.at[4 + k % nz], partner)
+
+    def d_own():
+        for side in (0, 1):
+            go(dy(1, side))
+
+    def d_turn():
+        for side in (0, 1):
+            dy_in(1, side).wait_recv()
+            go(dy(2, side))
+
+    def d_column():
+        for side in (0, 1):
+            dy_in(2, side).wait_recv()
+        go(d_core(0))
+
+    def d_send(*gs):
+        for side in (0, 1):
+            for g in gs:
+                go(dz(1, side, g))
+
+    def d_step(step, *gs):
+        for g in gs:
+            for side in (0, 1):
+                if step < nz // 2:
+                    dz_in(step, side, g).wait_recv()
+                    if step + 1 < nz // 2 or g in last_by[side]:
+                        go(dz(step + 1, side, g))
+                elif g in last_by[side]:
+                    dz_in(step, side, g).wait_recv()
+
+    def d_cores(step):
+        go(d_core(step))
+        if step < nz // 2:
+            go(d_core(-step))
+
+    def d_done():
+        for k in range(nz):
+            d_core_in(k).wait_recv()
+
+    deep = wo.shape[2]
+    wo_halves = (pl.ds(0, deep // 2), pl.ds(deep // 2, deep // 2))
+
+    def wx(step, side):
+        ref = wo.at[at_x(-fwd[side] * (step - 1)), c]
+        if step == 2:
+            ref = ref.at[wo_halves[side]]
+        return same(ref, wo_s.at[side, step - 1], wo_r.at[side, step - 1], x_to[side])
+
+    def wx_in(step, side):
+        ref = wo.at[at_x(-fwd[side] * step), c]
+        if step == 2:
+            ref = ref.at[wo_halves[side]]
+        return same(ref, wo_s.at[side, step - 1], wo_r.at[side, step - 1], x_to[side])
+
+    def w_core(i):
+        return same(wo.at[at_x(i + 1), c], core_s.at[12 + i], core_r.at[12 + i], partner)
+
+    def w_core_in(i):
+        return same(wo.at[at_x(i + 1), 1 - c], core_s.at[12 + i], core_r.at[12 + i], partner)
+
+    def w_turn():
+        for side in (0, 1):
+            wx_in(1, side).wait_recv()
+            go(wx(2, side))
+        go(w_core(0))
+        go(w_core(2))
+
+    def w_last():
+        for side in (0, 1):
+            wx_in(2, side).wait_recv()
+        go(w_core(1))
+
+    def w_done():
+        for i in range(nx - 1):
+            w_core_in(i).wait_recv()
+
+    for load in loads:
+        load.wait()
+    u_own()
+    d_own()
+    for side in (0, 1):
+        go(wx(1, side))
+
+    to_r = same(stream_all.at[x], st_s.at[0], st_r.at[0], right)
+    to_l = same(stream_all.at[x], st_s.at[1], st_r.at[1], left)
     to_r.start()
     to_l.start()
-    stream_all[pl.ds(x, 1)] = stream[...][None]
 
     lane = lax.broadcasted_iota(jnp.int32, (1, 128), 1)
     low = lane < HDN
@@ -121,6 +348,25 @@
     def spread(r):
         steps = jnp.minimum(columns[:, r : r + 1] - decays[pl.ds(r, 1), :], 0.0)
         return jnp.where(lower, jnp.exp(steps), 0.0)
+
+    def tick(b):
+        if b == 0:
+            d_turn()
+            d_send(0)
+        elif b == 1:
+            u_step(1)
+            d_column()
+        elif b == 2:
+            u_relay((0, 0))
+            d_send(1, 2)
+        elif b == 3:
+            u_step(2)
+            w_turn()
+        elif b == 4:
+            u_relay((1, 0), (1, 1))
+            d_send(3)
+        elif b == 5:
+            u_step(3)
 
     state_w = jnp.zeros((128, 128), F32)
     state_n = jnp.zeros((128, 128), F32)
@@ -176,6 +422,7 @@
         keep = jnp.where(low, jnp.exp(last[1]), jnp.exp(last[2]))
         state_n = keep * state_n + jnp.where(same_head, tdot(tail.astype(BF16), v), 0.0)
         gone = [g + t for g, t in zip(gone, last)]
+        tick(b)
 
     total_w = jnp.exp(gone[0]) + jnp.zeros((1, 128), F32)
     total_n = jnp.where(low, jnp.exp(gone[1]), jnp.exp(gone[2]))
@@ -196,19 +443,10 @@
         stage1(d).start()
     in1[pl.ds(me, 1)] = msg[pl.ds(me, 1)]
 
-    to_r.wait_recv()
-    on_r = remote(
-        stream_all.at[xl, pl.ds(0, half_rows)], stream_all.at[xl, pl.ds(0, half_rows)],
-        st_s.at[2], st_r.at[2], right,
-    )
-    on_r.start()
-    to_l.wait_recv()
-    on_l = remote(
-        stream_all.at[xr, pl.ds(half_rows, half_rows)], stream_all.at[xr, pl.ds(half_rows, half_rows)],
-        st_s.at[3], st_r.at[3], left,
-    )
-    on_l.start()
-
+    on_r = same(stream_all.at[xl, pl.ds(0, half_rows)], st_s.at[2], st_r.at[2], right)
+    on_l = same(stream_all.at[xr, pl.ds(half_rows, half_rows)], st_s.at[3], st_r.at[3], left)
+
+    d_step(1, 0)
     for d in range(1, plane):
         stage1(d).wait_recv()
     wide_row = lax.broadcasted_iota(jnp.int32, (ns, 128), 0) < sw
@@ -237,6 +475,8 @@
 
     for d in range(1, nz):
         stage2(d).start()
+    u_relay((2, 0), (2, 1))
+    u_step(4)
     in2[pl.ds(z, 1)] = tot2[...][None]
     for d in range(1, nz):
         stage2(d).wait_recv()
@@ -254,6 +494,7 @@
     for d in range(1, plane):
         stage3(d).start()
     in3[pl.ds(me, 1)] = msg3[pl.ds(me, 1)]
+    d_step(1, 1, 2)
     for d in range(1, plane):
         stage3(d).wait_recv()
     arrived = in3[...]
@@ -263,6 +504,11 @@
         [jnp.where(low, enter_p, 0.0), jnp.where(low, 0.0, enter_p)], axis=0
     ).astype(BF16)
 
+    u_relay((3, 0), (3, 1), (0, 1))
+    d_step(2, 0)
+    d_step(1, 3)
+    d_cores(1)
+
     def mixed_to(i, side):
         return remote(
             mixed.at[x, i], mixed.at[x, i], mx_s.at[side, i], mx_r.at[side, i], (right, left)[side]
@@ -295,6 +541,18 @@
         piece = mixed.at[src, i, pl.ds(start, half_rows)]
         return remote(piece, piece, mx_s.at[2 + side, i], mx_r.at[2 + side, i], (right, left)[side])
 
+    to_r.wait_recv()
+    on_r.start()
+    to_l.wait_recv()
+    on_l.start()
+    d_step(2, 1, 2)
+    u_rest()
+    w_last()
+    d_step(3, 0)
+    d_step(2, 3)
+    d_cores(2)
+    u_last()
+
     def pass_on(i, _):
         for side in (0, 1):
             mixed_to(i, side).wait_recv()
@@ -304,8 +562,9 @@
     lax.fori_loop(0, nx, pass_on, 0)
     on_r.wait_recv()
     on_l.wait_recv()
-
-    width = stream.shape[1]
+    w_done()
+    d_step(3, 1, 2)
+
     tile = 512
     tiles = width // tile
 
@@ -317,7 +576,7 @@
             at = pl.ds(pl.multiple_of(n * tile, tile), tile)
             total = stream_all[i, :, at].astype(F32)
             for j in range(nx):
-                total += dot(mixed[j, i], wo[j, :, at])
+                total += dot(mixed[j, i], wo[j, :, :, at].reshape(2 * deep, tile))
             total = total.astype(BF16)
             middle[i, :, at] = total
             total = total.astype(F32)
@@ -325,25 +584,37 @@
 
         squares = lax.fori_loop(0, tiles, project, jnp.zeros((rows, 1), F32))
         scale = lax.rsqrt(squares * (1.0 / width) + norm_eps)
-        normed[...] = (middle[i].astype(F32) * scale * gain[...].astype(F32)).astype(BF16)
-
-        def rise(n, _):
-            at = pl.ds(pl.multiple_of(n * tile, tile), tile)
-            h = jnp.maximum(dot(normed[...], up[:, at]), 0.0)
+        normed[i] = (middle[i].astype(F32) * scale * gain[...].astype(F32)).astype(BF16)
+        return 0
+
+    lax.fori_loop(0, nx, rows_in, 0)
+    d_step(3, 3)
+    d_cores(3)
+    u_done()
+
+    def rise(n, _):
+        at = pl.ds(pl.multiple_of(n * tile, tile), tile)
+
+        def one(i, _):
+            h = jnp.maximum(dot(normed[i], up[:, :, :, :, at].reshape(width, tile)), 0.0)
             hidden[i, :, at] = (h * h).astype(BF16)
             return 0
 
-        lax.fori_loop(0, tiles, rise, 0)
-        return 0
-
-    lax.fori_loop(0, nx, rows_in, 0)
+        return lax.fori_loop(0, nx, one, 0)
+
+    lax.fori_loop(0, tiles, rise, 0)
+    d_step(4, 0, 1, 2, 3)
+    d_cores(4)
+    d_done()
 
     side_tiles = tiles // 2
+    per_tile = nz // tiles
 
     def fall(i, side, into):
         def one(n, _):
             at = pl.ds(pl.multiple_of(n * tile, tile), tile)
-            part = dot_t(hidden[i], down[pl.ds(pl.multiple_of((side * side_tiles + n) * tile, tile), tile), :])
+            of_z = pl.ds((side * side_tiles + n) * per_tile, per_tile)
+            part = dot_t(hidden[i], down[of_z].reshape(tile, width))
             into[side, :, at] = part.astype(into.dtype)
             return 0
 
@@ -381,6 +652,8 @@
         total = own[s] + got_l[s].astype(F32) + got_r[s].astype(F32)
         out[:, at] = (middle[x, :, at].astype(F32) + total).astype(BF16)
 
+    for copy in sent:
+        copy.wait_send()
     for copy in (to_r, to_l, on_r, on_l, *far, *near_r, *near_l):
         copy.wait_send()
     for d in range(1, plane):
@@ -404,16 +677,12 @@
     tok = query_wide.shape[0]
     rows, width = stream_in.shape
     plane = ny * nc
-    sp_axes = ("z", "y", "c")
-    both = jnp.concatenate([up_weight, down_weight.T], axis=1)
-    both = lax.all_gather(both, sp_axes, axis=0, tiled=True)
-    hid = up_weight.shape[1]
-    up, down = both[:, :hid], both[:, hid:]
-    wo = lax.all_gather(jnp.concatenate([output_wide, output_narrow], axis=0), "x")
+    part, hid = up_weight.shape
     ns = (128 + HDN) // plane
     dma = pltpu.SemaphoreType.DMA
     vm = pltpu.VMEM
     scratch = [
+        vm((nz, ny, nc, part, hid), BF16), vm((nz, ny, nc, part, hid), BF16), vm((nx, 2, *output_wide.shape), BF16),
         vm((nx, rows, width), BF16),
         vm((tok, 128), BF16), vm((tok, 128), BF16), vm((tok, 128), F32), vm((tok, 128), F32),
         vm((128, 128), F32),
@@ -421,7 +690,7 @@
         vm((ns + 8, 128), F32), vm((nz, ns + 8, 128), F32),
         vm((plane, ns, 128), F32), vm((plane, ns, 128), F32),
         vm((nx, nx, rows, 256), BF16),
-        vm((nx, rows, width), BF16), vm((rows, width), BF16), vm((nx, rows, hid), BF16),
+        vm((nx, rows, width), BF16), vm((nx, rows, width), BF16), vm((nx, rows, hid), BF16),
         vm((2, rows, width // 2), BF16), vm((2, rows, width // 2), BF16), vm((2, rows, width // 2), BF16),
         vm((2, rows, width // 2), F32),
         vm((rows, width // 2), BF16), vm((rows, width // 2), BF16),
@@ -429,12 +698,15 @@
         dma((4,)), dma((4,)),
         dma((plane,)), dma((plane,)), dma((nz,)), dma((nz,)), dma((plane,)), dma((plane,)),
         dma((4, nx)), dma((4, nx)), dma((6,)), dma((6,)),
+        dma((5,)), dma((2, 2)), dma((2, 2)), dma((2, 4)), dma((2, 4)), dma((2, nz)), dma((2, nz)),
+        dma((2, 4)), dma((2, 4)), dma((2, 2)), dma((2, 2)), dma((2, 4, 4)), dma((2, 4, 4)), dma((15,)), dma((15,)),
     ]
     vmem = pl.BlockSpec(memory_space=pltpu.VMEM)
+    hbm = pl.BlockSpec(memory_space=pl.ANY)
     return pl.pallas_call(
         functools.partial(kernel, sizes),
         out_shape=jax.ShapeDtypeStruct((rows, width), BF16),
-        in_specs=[vmem] * 18,
+        in_specs=[hbm] + [vmem] * 14 + [hbm] * 4,
         out_specs=vmem,
         scratch_shapes=scratch,
         compiler_params=pltpu.CompilerParams(
@@ -444,7 +716,8 @@
         stream_in, query_wide, key_wide, value_wide, gate_wide, decay_wide,
         query_narrow, key_narrow, value_narrow, gate_narrow, decay_narrow,
         norm_gain[None], jnp.asarray(rope_tables(BLOCK, 1)), jnp.asarray(rope_tables(8, BLOCK)),
-        jnp.asarray(rope_tables(nz * plane, tok)), wo, up, down,
+        jnp.asarray(rope_tables(nz * plane, tok)),
+        output_wide, output_narrow, up_weight, down_weight.T,
     )
 
 

time: 276 us -> 134 us (0.49)
  waiting for transfers between devices: 139 us -> 0 us
  Pallas kernels: 103 us -> 130 us
  between operations: 13.4 us -> 0.01 us
  local copies, waits for them, and re-layouts: 15.4 us -> 3.38 us
  other arithmetic: 3.98 us -> 0 us
    all_gather x2 -> x0, waiting for transfers between devices: 139 us -> none  [the longest x1 102 us: on_device(): both = lax.all_gather(both, sp_axes, axis=0, tiled=True)]
    pallas_call x1, Pallas kernels: 103 us -> 130 us  [on_device(): pl.pallas_call(functools.partial(kernel, sizes), out_shape=jax.ShapeDtype...]
    slice x1 -> x0, local copies, waits for them, and re-layouts: 12 us -> none  [on_device(): up, down = (both[:, :hid], both[:, hid:])]
    concatenate x2 -> x0, other arithmetic: 3.98 us -> none  [the longest x1 2.29 us: on_device(): jnp.concatenate([output_wide, output_narrow], axis=0)]
  transfers between devices with their start and end apart: 2 -> 0, of which waited for: 2 -> 0; matrix products, arithmetic and copies ran while one was open for 6% -> 0% of each run, Pallas kernels for 0% -> 0%
where the time goes in v2:
time: 134 us
  Pallas kernels  130 us (97%)
  local copies, waits for them, and re-layouts  3.38 us (3%)
    pallas_call x1, Pallas kernels, on_device(): pl.pallas_call(functools.partial(kernel, sizes), out_shape=jax.ShapeDtype...  130 us

profile of v2, /device:TPU:1, one launch (start us, length us, event | category | flops | bytes accessed | tf_op | source)
XLA Modules:
  0.0 133.7 jit_solution(13544908097444800797)
XLA Ops:
  0.0 1.3 broadcast_in_dim.3.gain
  1.3 130.3 %shard_map.181 = bf16[192,2048]{1,0:T(8,128)(2,1)} custom-call(bf16[192,2048]{1,0:T(8,128)(2,1)} %stream.1, bf16[768,128]{1,0:T(8,128)(2,1)} %qw.1, bf16[768,128]{1,0:T(8,128)(2,1)} %kw.1, bf16[768,128]{1,0:T(8,128)(2,1)} %vw.1, bf16[768,128]{1,0:T(8,128)(2,1)} %gw.1, f32[1,768]{1,0:T(1,128)} %dw.1, bf16[768,128]{1,0:T(8,128)(2,1)} %qn.1, ...), custom_call_target="tpu_custom_call" | custom-call | tf_op jit(solution)/shard_map/pallas_call | solution.py:706
  131.6 2.1 %copy.21 = bf16[192,2048]{1,0:T(8,128)(2,1)} copy(bf16[192,2048]{1,0:T(8,128)(2,1)} %shard_map.181) | data formatting | bytes 1572864

commit v3 on v2

--- a/solution.py
+++ b/solution.py
@@ -55,11 +55,13 @@
 
 def kernel(
     sizes,
-    stream, qw, kw, vw, gw, dw, qn, kn, vn, gn, dn, gain, tt, tb, ts, ow, on, up_own, down_own,
+    dw, dn, gain, tt, tb, ts,
+    qw_in, kw_in, vw_in, qn_in, kn_in, vn_in, gw_in, gn_in, stream_in, ow, on, up_own, down_own,
     out,
+    qw, kw, vw, qn, kn, vn, gw, gn, stream,
     up, down, wo,
-    stream_all, qe_w, qe_n, o_w, o_n, decays, msg, in1, pre1, tot2, in2, msg3, in3,
-    mixed, middle, normed, hidden, send2, send1, sendm, own, relay_l, relay_r, got_l, got_r,
+    qe_w, qe_n, o_w, o_n, decays, msg, in1, tot2, in2, msg3, in3,
+    mixed, mix_in, middle, normed, hidden, send2, send1, sendm, own, relay_l, relay_r, got_l, got_r,
     st_s, st_r, s1_s, s1_r, s2_s, s2_r, s3_s, s3_r, mx_s, mx_r, rs_s, rs_r,
     in_s, wo_s, wo_r, uz_s, uz_r, uy_s, uy_r, ur_s, ur_r, dy_s, dy_r, dz_s, dz_r, core_s, core_r,
 ):
@@ -73,29 +75,37 @@
     blocks = tok // BLOCK
     rows = stream.shape[0]
     width = stream.shape[1]
-    half_rows = rows // 2
+    half_rows, part_rows = rows // 2, rows // 4
     right, left = {"x": xr}, {"x": xl}
 
     def at_plane(j):
         return {"y": j // nc, "c": lax.rem(j, nc)}
 
-    loads = [
-        pltpu.make_async_copy(up_own, up.at[z, y, c], in_s.at[0]),
-        pltpu.make_async_copy(down_own, down.at[z, y, c], in_s.at[1]),
-        pltpu.make_async_copy(ow, wo.at[x, 0], in_s.at[2]),
-        pltpu.make_async_copy(on, wo.at[x, 1], in_s.at[3]),
-        pltpu.make_async_copy(stream, stream_all.at[x], in_s.at[4]),
-    ]
-    for load in loads:
-        load.start()
-
     barrier = pltpu.get_barrier_semaphore()
-    peers = [right, left]
+    peers = [right, left, {"x": xo}]
     peers += [at_plane(lax.rem(me + d, plane)) for d in range(1, plane)]
     peers += [{"z": lax.rem(z + d, nz)} for d in range(1, nz)]
     for peer in peers:
         pl.semaphore_signal(barrier, inc=1, device_id=peer, device_id_type=MESH)
-    pl.semaphore_wait(barrier, len(peers))
+
+    pairs = [
+        (qw_in, qw), (kw_in, kw), (vw_in, vw), (qn_in, qn), (kn_in, kn), (vn_in, vn),
+        (up_own, up.at[z, y, c]), (ow, wo.at[x, 0]), (on, wo.at[x, 1]), (down_own, down.at[z, y, c]),
+        (gw_in, gw), (gn_in, gn), (stream_in, stream),
+    ]
+    loads = [pltpu.make_async_copy(a, b, in_s.at[i]) for i, (a, b) in enumerate(pairs)]
+    for load in loads:
+        load.start()
+
+    lane = lax.broadcasted_iota(jnp.int32, (1, 128), 1)
+    low = lane < HDN
+    base = []
+    for g in (0, 2):
+        row = [ts[g + i, pl.ds(sp, 1), :] for i in (0, 1)]
+        base.append(turn(row[0], row[1], tb[g], tb[g + 1]))
+    sign_w = jnp.where(lane < HDW // 2, -1.0, 1.0)
+    front_n = lax.rem(lane, HDN) < HDN // 2
+    sign_n = jnp.where(front_n, -1.0, 1.0)
 
     sent = []
 
@@ -172,6 +182,8 @@
             uz_in(step, side).wait_recv()
             if step < nz // 2:
                 go(uz(step + 1, side))
+
+    def u_turn(step):
         offs = (-step, step) if step < nz // 2 else (step,)
         for off in offs:
             for side in (0, 1):
@@ -272,16 +284,12 @@
     wo_halves = (pl.ds(0, deep // 2), pl.ds(deep // 2, deep // 2))
 
     def wx(step, side):
-        ref = wo.at[at_x(-fwd[side] * (step - 1)), c]
-        if step == 2:
-            ref = ref.at[wo_halves[side]]
-        return same(ref, wo_s.at[side, step - 1], wo_r.at[side, step - 1], x_to[side])
+        ref = wo.at[at_x(-fwd[side] if step == 2 else 0), c].at[wo_halves[1 - side if step == 1 else side]]
+        return same(ref, wo_s.at[side, step], wo_r.at[side, step], x_to[side])
 
     def wx_in(step, side):
-        ref = wo.at[at_x(-fwd[side] * step), c]
-        if step == 2:
-            ref = ref.at[wo_halves[side]]
-        return same(ref, wo_s.at[side, step - 1], wo_r.at[side, step - 1], x_to[side])
+        ref = wo.at[at_x(-fwd[side] * (2 if step == 2 else 1)), c].at[wo_halves[1 - side if step == 1 else side]]
+        return same(ref, wo_s.at[side, step], wo_r.at[side, step], x_to[side])
 
     def w_core(i):
         return same(wo.at[at_x(i + 1), c], core_s.at[12 + i], core_r.at[12 + i], partner)
@@ -291,8 +299,12 @@
 
     def w_turn():
         for side in (0, 1):
+            wx_in(0, side).wait_recv()
+            go(wx(2, side))
+
+    def w_near():
+        for side in (0, 1):
             wx_in(1, side).wait_recv()
-            go(wx(2, side))
         go(w_core(0))
         go(w_core(2))
 
@@ -305,27 +317,8 @@
         for i in range(nx - 1):
             w_core_in(i).wait_recv()
 
-    for load in loads:
+    for load in loads[:6]:
         load.wait()
-    u_own()
-    d_own()
-    for side in (0, 1):
-        go(wx(1, side))
-
-    to_r = same(stream_all.at[x], st_s.at[0], st_r.at[0], right)
-    to_l = same(stream_all.at[x], st_s.at[1], st_r.at[1], left)
-    to_r.start()
-    to_l.start()
-
-    lane = lax.broadcasted_iota(jnp.int32, (1, 128), 1)
-    low = lane < HDN
-    base = []
-    for g in (0, 2):
-        row = [ts[g + i, pl.ds(sp, 1), :] for i in (0, 1)]
-        base.append(turn(row[0], row[1], tb[g], tb[g + 1]))
-    sign_w = jnp.where(lane < HDW // 2, -1.0, 1.0)
-    front_n = lax.rem(lane, HDN) < HDN // 2
-    sign_n = jnp.where(front_n, -1.0, 1.0)
 
     decays[...] = jnp.zeros_like(decays)
     for b in range(blocks):
@@ -348,25 +341,6 @@
     def spread(r):
         steps = jnp.minimum(columns[:, r : r + 1] - decays[pl.ds(r, 1), :], 0.0)
         return jnp.where(lower, jnp.exp(steps), 0.0)
-
-    def tick(b):
-        if b == 0:
-            d_turn()
-            d_send(0)
-        elif b == 1:
-            u_step(1)
-            d_column()
-        elif b == 2:
-            u_relay((0, 0))
-            d_send(1, 2)
-        elif b == 3:
-            u_step(2)
-            w_turn()
-        elif b == 4:
-            u_relay((1, 0), (1, 1))
-            d_send(3)
-        elif b == 5:
-            u_step(3)
 
     state_w = jnp.zeros((128, 128), F32)
     state_n = jnp.zeros((128, 128), F32)
@@ -422,31 +396,43 @@
         keep = jnp.where(low, jnp.exp(last[1]), jnp.exp(last[2]))
         state_n = keep * state_n + jnp.where(same_head, tdot(tail.astype(BF16), v), 0.0)
         gone = [g + t for g, t in zip(gone, last)]
-        tick(b)
 
     total_w = jnp.exp(gone[0]) + jnp.zeros((1, 128), F32)
     total_n = jnp.where(low, jnp.exp(gone[1]), jnp.exp(gone[2]))
     packed_n = jnp.where(low, state_n[:HDN], state_n[HDN:])
     sw, sn = 128 // plane, HDN // plane
+    part_of = lax.broadcasted_iota(jnp.int32, (8, 128), 0)
+
+    def message(state, rate_w, rate_n):
+        parts = jnp.zeros((8, 128), F32)
+        for r, rate in ((0, rate_w), (2, rate_n)):
+            high = rate.astype(BF16).astype(F32)
+            parts = jnp.where(part_of == r, high, jnp.where(part_of == r + 1, rate - high, parts))
+        return jnp.concatenate([state, parts], axis=0).astype(BF16)
+
     for j in range(plane):
-        msg[j, 0:sw, :] = state_w[sw * j : sw * (j + 1)]
-        msg[j, sw : sw + sn, :] = packed_n[sn * j : sn * (j + 1)]
-        msg[j, sw + sn : sw + sn + 1, :] = total_w
-        msg[j, sw + sn + 1 : sw + sn + 2, :] = total_n
+        state = [state_w[sw * j : sw * (j + 1)], packed_n[sn * j : sn * (j + 1)]]
+        msg[j] = message(jnp.concatenate(state, axis=0), total_w, total_n)
     ns = sw + sn
 
     def stage1(d):
         to = lax.rem(me + d, plane)
         return remote(msg.at[to], in1.at[me], s1_s.at[d], s1_r.at[d], at_plane(to))
 
+    pl.semaphore_wait(barrier, len(peers))
     for d in range(1, plane):
         stage1(d).start()
+    for load in loads[6:10]:
+        load.wait()
+    for side in (0, 1):
+        go(uz(1, side))
+        go(wx(0, side))
+    d_own()
+    for side in (0, 1):
+        go(wx(1, side))
+    d_send(0)
     in1[pl.ds(me, 1)] = msg[pl.ds(me, 1)]
 
-    on_r = same(stream_all.at[xl, pl.ds(0, half_rows)], st_s.at[2], st_r.at[2], right)
-    on_l = same(stream_all.at[xr, pl.ds(half_rows, half_rows)], st_s.at[3], st_r.at[3], left)
-
-    d_step(1, 0)
     for d in range(1, plane):
         stage1(d).wait_recv()
     wide_row = lax.broadcasted_iota(jnp.int32, (ns, 128), 0) < sw
@@ -454,38 +440,43 @@
     def factor(pair):
         return jnp.where(wide_row, pair[0], pair[1])
 
-    def rates(ref, j):
-        return ref[j, ns : ns + 1, :], ref[j, ns + 1 : ns + 2, :]
-
+    def opened(ref, j):
+        whole = ref[j].astype(F32)
+        return whole[0:ns], (whole[ns : ns + 1] + whole[ns + 1 : ns + 2], whole[ns + 2 : ns + 3] + whole[ns + 3 : ns + 4])
+
+    before = []
     held = jnp.zeros((ns, 128), F32)
     rate = (jnp.ones((1, 128), F32), jnp.ones((1, 128), F32))
     for j in range(plane):
-        pre1[j, 0:ns, :] = held
-        pre1[j, ns : ns + 1, :] = rate[0]
-        pre1[j, ns + 1 : ns + 2, :] = rate[1]
-        mine = rates(in1, j)
-        held = held * factor(mine) + in1[j, 0:ns, :]
+        before.append((held, rate))
+        state, mine = opened(in1, j)
+        held = held * factor(mine) + state
         rate = (rate[0] * mine[0], rate[1] * mine[1])
-    tot2[0:ns, :] = held
-    tot2[ns : ns + 1, :] = rate[0]
-    tot2[ns + 1 : ns + 2, :] = rate[1]
+    tot2[...] = message(held, *rate)
 
     def stage2(d):
         return remote(tot2, in2.at[z], s2_s.at[d], s2_r.at[d], {"z": lax.rem(z + d, nz)})
 
     for d in range(1, nz):
         stage2(d).start()
-    u_relay((2, 0), (2, 1))
-    u_step(4)
+    for side in (0, 1):
+        go(uy(0, side))
+    u_step(1)
+    d_turn()
+    d_send(1)
+    w_turn()
     in2[pl.ds(z, 1)] = tot2[...][None]
     for d in range(1, nz):
         stage2(d).wait_recv()
     held = jnp.zeros((ns, 128), F32)
     for k in range(nz):
-        later = held * factor(rates(in2, k)) + in2[k, 0:ns, :]
+        state, mine = opened(in2, k)
+        later = held * factor(mine) + state
         held = jnp.where(k < z, later, held)
     for j in range(plane):
-        msg3[j] = held * factor(rates(pre1, j)) + pre1[j, 0:ns, :]
+        state, rate = before[j]
+        state = held * factor(rate) + state
+        msg3[j] = jnp.concatenate([state, jnp.zeros((8, 128), F32)], axis=0).astype(BF16)
 
     def stage3(d):
         to = lax.rem(me + d, plane)
@@ -494,25 +485,24 @@
     for d in range(1, plane):
         stage3(d).start()
     in3[pl.ds(me, 1)] = msg3[pl.ds(me, 1)]
-    d_step(1, 1, 2)
+    u_turn(1)
+    d_column()
+    u_step(2)
+    d_send(2)
+    for load in loads[10:]:
+        load.wait()
     for d in range(1, plane):
         stage3(d).wait_recv()
-    arrived = in3[...]
+    arrived = in3[...].astype(F32)
     enter_w = arrived[:, 0:sw, :].reshape(128, 128).astype(BF16)
     enter_p = arrived[:, sw:ns, :].reshape(HDN, 128)
     enter_n = jnp.concatenate(
         [jnp.where(low, enter_p, 0.0), jnp.where(low, 0.0, enter_p)], axis=0
     ).astype(BF16)
 
-    u_relay((3, 0), (3, 1), (0, 1))
-    d_step(2, 0)
-    d_step(1, 3)
-    d_cores(1)
-
-    def mixed_to(i, side):
-        return remote(
-            mixed.at[x, i], mixed.at[x, i], mx_s.at[side, i], mx_r.at[side, i], (right, left)[side]
-        )
+    def mixed_to(d):
+        to = lax.rem(x + d, nx)
+        return remote(mixed.at[to], mix_in.at[x], mx_s.at[d], mx_r.at[d], {"x": to})
 
     def gated(o, gate):
         return (o * jax.nn.silu(gate.astype(F32))).astype(BF16)
@@ -522,7 +512,7 @@
         o = o_w[cut, :] + dot(qe_w[cut, :], enter_w)
         o = o - jnp.mean(o, axis=-1, keepdims=True)
         o = o * lax.rsqrt(jnp.mean(o * o, axis=-1, keepdims=True) + head_eps)
-        mixed[x, i, :, 0:128] = gated(o, gw[cut, :])
+        mixed[i, :, 0:128] = gated(o, gw[cut, :])
         o = o_n[cut, :] + dot(qe_n[cut, :], enter_n)
 
         def by_head(a):
@@ -532,93 +522,104 @@
 
         o = o - by_head(o)
         o = o * lax.rsqrt(by_head(o * o) + head_eps)
-        mixed[x, i, :, 128:256] = gated(o, gn[cut, :])
-        mixed_to(i, 0).start()
-        mixed_to(i, 1).start()
-
-    def mixed_on(i, side):
-        src, start = ((xl, 0), (xr, half_rows))[side]
-        piece = mixed.at[src, i, pl.ds(start, half_rows)]
-        return remote(piece, piece, mx_s.at[2 + side, i], mx_r.at[2 + side, i], (right, left)[side])
-
-    to_r.wait_recv()
-    on_r.start()
-    to_l.wait_recv()
-    on_l.start()
-    d_step(2, 1, 2)
-    u_rest()
+        mixed[i, :, 128:256] = gated(o, gn[cut, :])
+
+    for d in (2, 1, 3):
+        go(mixed_to(d))
+    mix_in[pl.ds(x, 1)] = mixed[pl.ds(x, 1)]
+
+    u_turn(2)
+    u_relay((0, 0))
+    w_near()
+    u_step(3)
+    u_turn(3)
+    d_send(3)
+    d_step(1, 0, 1)
     w_last()
-    d_step(3, 0)
+    w_done()
+    u_relay((1, 0), (1, 1))
+    for d in (1, 3, 2):
+        mixed_to(d).wait_recv()
+
+    tile = 512
+    tiles = width // tile
+
+    def project(n, squares):
+        at = pl.ds(pl.multiple_of(n * tile, tile), tile)
+        total = stream[:, at].astype(F32)
+        for j in range(nx):
+            total += dot(mix_in[j], wo[j, :, :, at].reshape(2 * deep, tile))
+        total = total.astype(BF16)
+        middle[:, at] = total
+        total = total.astype(F32)
+        return squares + jnp.sum(total * total, axis=-1, keepdims=True)
+
+    squares = lax.fori_loop(0, tiles, project, jnp.zeros((rows, 1), F32))
+    scale = lax.rsqrt(squares * (1.0 / width) + norm_eps)
+    normed[pl.ds(x, 1)] = (middle[...].astype(F32) * scale * gain[...].astype(F32).reshape(1, width)).astype(BF16)[None]
+
+    def nx_rows(piece, side):
+        start = side * half_rows if piece in (0, 3) else (1 - side) * half_rows + (piece - 1) * part_rows
+        return pl.ds(start, half_rows if piece in (0, 3) else part_rows)
+
+    def nm(piece, side):
+        ref = normed.at[at_x(-fwd[side] if piece == 3 else 0), nx_rows(piece, side)]
+        return same(ref, st_s.at[side, piece], st_r.at[side, piece], x_to[side])
+
+    def nm_in(piece, side):
+        ref = normed.at[at_x(-fwd[side] * (2 if piece == 3 else 1)), nx_rows(piece, side)]
+        return same(ref, st_s.at[side, piece], st_r.at[side, piece], x_to[side])
+
+    for piece in (0, 1):
+        for side in (0, 1):
+            go(nm(piece, side))
+
+    d_step(1, 2)
+    u_step(4)
+    u_turn(4)
+    u_relay((2, 1), (2, 0))
+    d_step(1, 3)
+    d_cores(1)
+    d_step(2, 0, 1)
+    u_relay((3, 1))
+    d_step(2, 2)
+    for side in (0, 1):
+        nm_in(0, side).wait_recv()
+        go(nm(3, side))
+        go(nm(2, side))
+    u_relay((3, 0), (0, 1))
     d_step(2, 3)
     d_cores(2)
+    u_rest()
+    d_step(3, 0, 1)
     u_last()
-
-    def pass_on(i, _):
-        for side in (0, 1):
-            mixed_to(i, side).wait_recv()
-            mixed_on(i, side).start()
-        return 0
-
-    lax.fori_loop(0, nx, pass_on, 0)
-    on_r.wait_recv()
-    on_l.wait_recv()
-    w_done()
-    d_step(3, 1, 2)
-
-    tile = 512
-    tiles = width // tile
-
-    def rows_in(i, _):
-        mixed_on(i, 0).wait_recv()
-        mixed_on(i, 1).wait_recv()
-
-        def project(n, squares):
-            at = pl.ds(pl.multiple_of(n * tile, tile), tile)
-            total = stream_all[i, :, at].astype(F32)
-            for j in range(nx):
-                total += dot(mixed[j, i], wo[j, :, :, at].reshape(2 * deep, tile))
-            total = total.astype(BF16)
-            middle[i, :, at] = total
-            total = total.astype(F32)
-            return squares + jnp.sum(total * total, axis=-1, keepdims=True)
-
-        squares = lax.fori_loop(0, tiles, project, jnp.zeros((rows, 1), F32))
-        scale = lax.rsqrt(squares * (1.0 / width) + norm_eps)
-        normed[i] = (middle[i].astype(F32) * scale * gain[...].astype(F32)).astype(BF16)
-        return 0
-
-    lax.fori_loop(0, nx, rows_in, 0)
+    d_step(3, 2)
+    u_done()
     d_step(3, 3)
     d_cores(3)
-    u_done()
-
-    def rise(n, _):
-        at = pl.ds(pl.multiple_of(n * tile, tile), tile)
-
-        def one(i, _):
+
+    def rise(i):
+        def one(n, _):
+            at = pl.ds(pl.multiple_of(n * tile, tile), tile)
             h = jnp.maximum(dot(normed[i], up[:, :, :, :, at].reshape(width, tile)), 0.0)
             hidden[i, :, at] = (h * h).astype(BF16)
             return 0
 
-        return lax.fori_loop(0, nx, one, 0)
-
-    lax.fori_loop(0, tiles, rise, 0)
-    d_step(4, 0, 1, 2, 3)
-    d_cores(4)
-    d_done()
+        lax.fori_loop(0, tiles, one, 0)
+
+    for side in (0, 1):
+        nm_in(3, side).wait_recv()
+    rise(xo)
 
     side_tiles = tiles // 2
-    per_tile = nz // tiles
+    by_distance = (0, 1, -1, 2, -2, 3, -3, 4)
+    span = width // nz
 
     def fall(i, side, into):
-        def one(n, _):
-            at = pl.ds(pl.multiple_of(n * tile, tile), tile)
-            of_z = pl.ds((side * side_tiles + n) * per_tile, per_tile)
-            part = dot_t(hidden[i], down[of_z].reshape(tile, width))
-            into[side, :, at] = part.astype(into.dtype)
-            return 0
-
-        lax.fori_loop(0, side_tiles, one, 0)
+        for n in range(nz // 2):
+            of_z = at_z(by_distance[side * (nz // 2) + n])
+            piece = dot_t(hidden[i], down[of_z].reshape(span, width))
+            into[side, :, n * span : (n + 1) * span] = piece.astype(into.dtype)
 
     far = [
         remote(send2.at[0], relay_l, rs_s.at[0], rs_r.at[0], right),
@@ -626,12 +627,23 @@
     ]
     near_r = [remote(send1.at[s], got_l.at[s], rs_s.at[2 + s], rs_r.at[2 + s], right) for s in (0, 1)]
     near_l = [remote(sendm.at[s], got_r.at[s], rs_s.at[4 + s], rs_r.at[4 + s], left) for s in (0, 1)]
+    for k in (0, 1, -1, 2):
+        d_core_in(k).wait_recv()
     fall(xo, 0, send2)
     far[0].start()
+    d_step(4, 0, 1, 2, 3)
+    d_cores(4)
+    for k in (-2, 3, -3, 4):
+        d_core_in(k).wait_recv()
     fall(xo, 1, send2)
     far[1].start()
+    for side in (0, 1):
+        for piece in (1, 2):
+            nm_in(piece, side).wait_recv()
+    rise(xr)
     fall(xr, 1, send1)
     near_r[1].start()
+    rise(xl)
     fall(xl, 0, sendm)
     near_l[0].start()
     fall(xr, 0, own)
@@ -642,29 +654,26 @@
     far[1].wait_recv()
     sendm[1] = (own[1] + relay_r[...].astype(F32)).astype(BF16)
     near_l[1].start()
+    rise(x)
     fall(x, 0, own)
     fall(x, 1, own)
-    span = width // 2
     for s, first, second in ((1, near_r, near_l), (0, near_l, near_r)):
         first[s].wait_recv()
         second[s].wait_recv()
-        at = slice(s * span, (s + 1) * span)
         total = own[s] + got_l[s].astype(F32) + got_r[s].astype(F32)
-        out[:, at] = (middle[x, :, at].astype(F32) + total).astype(BF16)
+        for n in range(nz // 2):
+            at = pl.ds(pl.multiple_of(at_z(by_distance[s * (nz // 2) + n]) * span, span), span)
+            out[:, at] = (middle[:, at].astype(F32) + total[:, n * span : (n + 1) * span]).astype(BF16)
 
     for copy in sent:
         copy.wait_send()
-    for copy in (to_r, to_l, on_r, on_l, *far, *near_r, *near_l):
+    for copy in (*far, *near_r, *near_l):
         copy.wait_send()
     for d in range(1, plane):
         stage1(d).wait_send()
         stage3(d).wait_send()
     for d in range(1, nz):
         stage2(d).wait_send()
-    for i in range(nx):
-        for side in (0, 1):
-            mixed_to(i, side).wait_send()
-            mixed_on(i, side).wait_send()
 
 
 def on_device(
@@ -682,23 +691,23 @@
     dma = pltpu.SemaphoreType.DMA
     vm = pltpu.VMEM
     scratch = [
+        *[vm((tok, 128), BF16)] * 8, vm((rows, width), BF16),
         vm((nz, ny, nc, part, hid), BF16), vm((nz, ny, nc, part, hid), BF16), vm((nx, 2, *output_wide.shape), BF16),
-        vm((nx, rows, width), BF16),
         vm((tok, 128), BF16), vm((tok, 128), BF16), vm((tok, 128), F32), vm((tok, 128), F32),
         vm((128, 128), F32),
-        vm((plane, ns + 8, 128), F32), vm((plane, ns + 8, 128), F32), vm((plane, ns + 8, 128), F32),
-        vm((ns + 8, 128), F32), vm((nz, ns + 8, 128), F32),
-        vm((plane, ns, 128), F32), vm((plane, ns, 128), F32),
-        vm((nx, nx, rows, 256), BF16),
-        vm((nx, rows, width), BF16), vm((nx, rows, width), BF16), vm((nx, rows, hid), BF16),
+        vm((plane, ns + 8, 128), BF16), vm((plane, ns + 8, 128), BF16),
+        vm((ns + 8, 128), BF16), vm((nz, ns + 8, 128), BF16),
+        vm((plane, ns + 8, 128), BF16), vm((plane, ns + 8, 128), BF16),
+        vm((nx, rows, 256), BF16), vm((nx, rows, 256), BF16),
+        vm((rows, width), BF16), vm((nx, rows, width), BF16), vm((nx, rows, hid), BF16),
         vm((2, rows, width // 2), BF16), vm((2, rows, width // 2), BF16), vm((2, rows, width // 2), BF16),
         vm((2, rows, width // 2), F32),
         vm((rows, width // 2), BF16), vm((rows, width // 2), BF16),
         vm((2, rows, width // 2), BF16), vm((2, rows, width // 2), BF16),
-        dma((4,)), dma((4,)),
+        dma((2, 4)), dma((2, 4)),
         dma((plane,)), dma((plane,)), dma((nz,)), dma((nz,)), dma((plane,)), dma((plane,)),
-        dma((4, nx)), dma((4, nx)), dma((6,)), dma((6,)),
-        dma((5,)), dma((2, 2)), dma((2, 2)), dma((2, 4)), dma((2, 4)), dma((2, nz)), dma((2, nz)),
+        dma((nx,)), dma((nx,)), dma((6,)), dma((6,)),
+        dma((13,)), dma((2, 3)), dma((2, 3)), dma((2, 4)), dma((2, 4)), dma((2, nz)), dma((2, nz)),
         dma((2, 4)), dma((2, 4)), dma((2, 2)), dma((2, 2)), dma((2, 4, 4)), dma((2, 4, 4)), dma((15,)), dma((15,)),
     ]
     vmem = pl.BlockSpec(memory_space=pltpu.VMEM)
@@ -706,17 +715,16 @@
     return pl.pallas_call(
         functools.partial(kernel, sizes),
         out_shape=jax.ShapeDtypeStruct((rows, width), BF16),
-        in_specs=[hbm] + [vmem] * 14 + [hbm] * 4,
+        in_specs=[vmem] * 6 + [hbm] * 13,
         out_specs=vmem,
         scratch_shapes=scratch,
         compiler_params=pltpu.CompilerParams(
             collective_id=0, has_side_effects=True, vmem_limit_bytes=60 * 1024 * 1024
         ),
     )(
-        stream_in, query_wide, key_wide, value_wide, gate_wide, decay_wide,
-        query_narrow, key_narrow, value_narrow, gate_narrow, decay_narrow,
-        norm_gain[None], jnp.asarray(rope_tables(BLOCK, 1)), jnp.asarray(rope_tables(8, BLOCK)),
-        jnp.asarray(rope_tables(nz * plane, tok)),
+        decay_wide, decay_narrow, norm_gain, jnp.asarray(rope_tables(BLOCK, 1)),
+        jnp.asarray(rope_tables(8, BLOCK)), jnp.asarray(rope_tables(nz * plane, tok)),
+        query_wide, key_wide, value_wide, query_narrow, key_narrow, value_narrow, gate_wide, gate_narrow, stream_in,
         output_wide, output_narrow, up_weight, down_weight.T,
     )
 

time: 134 us -> 102 us (0.76)
  Pallas kernels: 130 us -> 99.4 us
    pallas_call x1, Pallas kernels: 130 us -> 99.4 us  [on_device(): pl.pallas_call(functools.partial(kernel, sizes), out_shape=jax.ShapeDtype...]
where the time goes in v3:
time: 102 us
  Pallas kernels  99.4 us (97%)
  local copies, waits for them, and re-layouts  2.09 us (2%)
    pallas_call x1, Pallas kernels, on_device(): pl.pallas_call(functools.partial(kernel, sizes), out_shape=jax.ShapeDtype...  99.4 us
    unnamed x1, local copies, waits for them, and re-layouts  2.09 us

profile of v3, /device:TPU:1, one launch (start us, length us, event | category | flops | bytes accessed | tf_op | source)
XLA Modules:
  0.0 101.5 jit_solution(8953314346942808842)
XLA Ops:
  0.0 99.4 %shard_map.181 = bf16[192,2048]{1,0:T(8,128)(2,1)} custom-call(f32[1,768]{1,0:T(1,128)} %dw.1, f32[2,768]{1,0:T(2,128)} %dn.1, bf16[2048]{0:T(1024)(128)(2,1)} %gain.1, f32[4,128,128]{2,1,0:T(8,128)} %constant.6.clone.tt, f32[4,8,128]{2,1,0:T(8,128)} %constant.7.clone.tb, f32[4,64,128]{2,1,0:T(8,128)} %constant.8.clone.ts, bf16[768,128]{1,0:T(8,128)(2,1)} %qw_in.1, ...), custom_call_target="tpu_custom_call" | custom-call | tf_op jit(solution)/shard_map/pallas_call | solution.py:715
  99.4 2.1 %copy.21 = bf16[192,2048]{1,0:T(8,128)(2,1)} copy(bf16[192,2048]{1,0:T(8,128)(2,1)} %shard_map.181) | data formatting | bytes 1572864

commit v4 on v3

v4 whole, which is shorter than its diff:
```python
import functools

import jax
import jax.numpy as jnp
import numpy as np
from jax import lax
from jax.experimental import pallas as pl
from jax.experimental.pallas import tpu as pltpu
from jax.sharding import Mesh
from jax.sharding import PartitionSpec as P

HDW = 128
HDN = 64
BLOCK = 128
head_eps = 1e-05
norm_eps = 1e-06
rope_base = 10000.0
MESH = pl.DeviceIdType.MESH
F32 = jnp.float32
BF16 = jnp.bfloat16


def rope_tables(steps, stride):
    tables = []
    for width in (HDW, HDN):
        half = width // 2
        inverse = rope_base ** (-np.arange(half, dtype=np.float64) / half)
        lanes = np.tile(inverse, 128 // half)
        angles = (stride * np.arange(steps, dtype=np.float64))[:, None] * lanes[None, :]
        tables += [np.cos(angles), np.sin(angles)]
    return np.stack(tables).astype(np.float32)


def remote(src, dst, send_sem, recv_sem, device):
    return pltpu.make_async_remote_copy(
        src_ref=src, dst_ref=dst, send_sem=send_sem, recv_sem=recv_sem, device_id=device, device_id_type=MESH
    )


def turn(cos_a, sin_a, cos_b, sin_b):
    return cos_a * cos_b - sin_a * sin_b, sin_a * cos_b + cos_a * sin_b


def dot(a, b):
    return jnp.dot(a, b, preferred_element_type=F32)


def dot_t(a, b):
    return lax.dot_general(a, b, (((1,), (1,)), ((), ())), preferred_element_type=F32)


def tdot(a, b):
    return lax.dot_general(a, b, (((0,), (0,)), ((), ())), preferred_element_type=F32)


def kernel(
    sizes,
    dw, dn, gain, tt, tb, ts,
    qw_in, kw_in, vw_in, qn_in, kn_in, vn_in, gw_in, gn_in, stream_in, ow, on, up_own, down_own,
    out,
    qw, kw, vw, qn, kn, vn, gw, gn, stream,
    up, down, wo,
    qe_w, qe_n, o_w, o_n, decays, st_w, st_n, k_w, k_n, msg, in1, tot2, in2, msg3, in3,
    mixed, mix_in, middle, normed, hidden, send2, send1, sendm, own, hold, result, relay_l, relay_r, got_both,
    left_s, in_s, out_s, st_r, s1_r, s2_r, s3_r, mx_r, rs_r, wo_r, uz_r, uy_r, ur_r, dy_r, dz_r, core_r,
):
    nz, ny, nc, nx = sizes
    z, y, c, x = (lax.axis_index(a) for a in ("z", "y", "c", "x"))
    xr, xl, xo = lax.rem(x + 1, nx), lax.rem(x + nx - 1, nx), lax.rem(x + 2, nx)
    plane = ny * nc
    me = y * nc + c
    sp = z * plane + me
    tok = qw.shape[0]
    blocks = tok // BLOCK
    rows = stream.shape[0]
    width = stream.shape[1]
    half_rows, few = rows // 2, rows // 6
    right, left = {"x": xr}, {"x": xl}

    def at_plane(j):
        return {"y": j // nc, "c": lax.rem(j, nc)}

    barrier = pltpu.get_barrier_semaphore()
    peers = [right, left, {"x": xo}]
    peers += [at_plane(lax.rem(me + d, plane)) for d in range(1, plane)]
    peers += [{"z": lax.rem(z + d, nz)} for d in range(1, nz)]
    for peer in peers:
        pl.semaphore_signal(barrier, inc=1, device_id=peer, device_id_type=MESH)

    pairs = [
        (kw_in, kw), (vw_in, vw), (kn_in, kn), (vn_in, vn),
        (up_own, up.at[z, y, c]), (ow, wo.at[x, 0]), (on, wo.at[x, 1]), (down_own, down.at[z, y, c]),
        (qw_in, qw), (qn_in, qn), (gw_in, gw), (gn_in, gn), (stream_in, stream),
    ]
    loads = [pltpu.make_async_copy(a, b, in_s.at[i]) for i, (a, b) in enumerate(pairs)]
    for load in loads:
        load.start()

    lane = lax.broadcasted_iota(jnp.int32, (1, 128), 1)
    low = lane < HDN
    base = []
    for g in (0, 2):
        row = [ts[g + i, pl.ds(sp, 1), :] for i in (0, 1)]
        base.append(turn(row[0], row[1], tb[g], tb[g + 1]))
    sign_w = jnp.where(lane < HDW // 2, -1.0, 1.0)
    front_n = lax.rem(lane, HDN) < HDN // 2
    sign_n = jnp.where(front_n, -1.0, 1.0)

    def go(copy):
        copy.start()

    def wait_all(ref, sem):
        pltpu.make_async_copy(ref, ref, sem).wait()

    def same(ref, send_sem, recv_sem, device):
        return remote(ref, ref, send_sem, recv_sem, device)

    z_to = ({"z": lax.rem(z + 1, nz)}, {"z": lax.rem(z + nz - 1, nz)})
    y_to = ({"y": lax.rem(y + 1, ny)}, {"y": lax.rem(y + ny - 1, ny)})
    x_to = (right, left)
    partner = {"c": 1 - c}
    fwd = (1, -1)

    def at_z(k):
        return lax.rem(z + nz + k, nz)

    def at_y(k):
        return lax.rem(y + ny + k, ny)

    def at_x(k):
        return lax.rem(x + nx + k, nx)

    part = up.shape[3]
    halves = (pl.ds(0, part // 2), pl.ds(part // 2, part // 2))

    relayed = ((0, 1, 2, 3), (4, -1, -2, -3))

    def uz(step, side):
        ref = up.at[at_z(-fwd[side] * (step - 1)), y, c]
        if step == nz // 2:
            ref = ref.at[halves[side]]
        return same(ref, left_s.at[0], uz_r.at[side, step - 1], z_to[side])

    def uz_in(step, side):
        ref = up.at[at_z(-fwd[side] * step), y, c]
        if step == nz // 2:
            ref = ref.at[halves[side]]
        return same(ref, left_s.at[0], uz_r.at[side, step - 1], z_to[side])

    def uy(off, side):
        return same(up.at[at_z(off), y, c], left_s.at[1], uy_r.at[side, relayed[side].index(off) if off in relayed[side] else 4], y_to[side])

    def uy_in(off, side):
        ref = up.at[at_z(off), at_y(-fwd[side]), c]
        return same(ref, left_s.at[1], uy_r.at[side, relayed[side].index(off) if off in relayed[side] else 4], y_to[side])


    def ur(i, side):
        ref = up.at[at_z(relayed[side][i]), at_y(-fwd[side]), c]
        return same(ref, left_s.at[2], ur_r, y_to[side])

    def u_core(i):
        ref = up.at[:, at_y((0, 1, -1, 2)[i]), c]
        return same(ref, left_s.at[6], core_r.at[0], partner)

    def u_step(step):
        for side in (0, 1):
            uz_in(step, side).wait_recv()
            if step < nz // 2:
                go(uz(step + 1, side))

    def u_turn(step):
        offs = (-step, step) if step < nz // 2 else (step,)
        for off in offs:
            for side in (0, 1):
                go(uy(off, side))
        if step == nz // 2:
            go(u_core(0))

    def u_relay(*which):
        for i, side in which:
            uy_in(relayed[side][i], side).wait_recv()
            go(ur(i, side))

    def u_rest():
        for side in (0, 1):
            wait_all(up.at[pl.ds(0, 4), 0, 0], uy_r.at[side, 4])
        go(u_core(1))
        go(u_core(2))

    def u_last():
        wait_all(up.at[:, 0, 0], ur_r)
        go(u_core(3))

    def u_done():
        wait_all(up.at[:, :, 0], core_r.at[0])

    by_distance = (0, 1, -1, 2, -2, 3, -3, 4)
    early = 5

    def dy(step, side):
        ref = down.at[z, at_y(-fwd[side] * (step - 1)), c]
        if step == 2:
            ref = ref.at[halves[side]]
        return same(ref, left_s.at[3], dy_r.at[side, step - 1], y_to[side])

    def dy_in(step, side):
        ref = down.at[z, at_y(-fwd[side] * step), c]
        if step == 2:
            ref = ref.at[halves[side]]
        return same(ref, left_s.at[3], dy_r.at[side, step - 1], y_to[side])

    columns_y = (0, 1, -1, 2)
    last_by = ((0, 3), (2, 1))

    def dz(step, side, g):
        ref = down.at[at_z(-fwd[side] * (step - 1)), at_y(columns_y[g]), c]
        return same(ref, left_s.at[4], dz_r.at[side, step - 1, g], z_to[side])

    def dz_in(step, side, g):
        ref = down.at[at_z(-fwd[side] * step), at_y(columns_y[g]), c]
        return same(ref, left_s.at[4], dz_r.at[side, step - 1, g], z_to[side])

    def d_core(k):
        return same(down.at[at_z(k), :, c], left_s.at[6], core_r.at[2 if k in by_distance[:early] else 3], partner)

    def d_own():
        for side in (0, 1):
            go(dy(1, side))

    def d_turn():
        for side in (0, 1):
            dy_in(1, side).wait_recv()
            go(dy(2, side))

    def d_column():
        for side in (0, 1):
            dy_in(2, side).wait_recv()
        go(d_core(0))

    def d_send(*gs):
        for side in (0, 1):
            for g in gs:
                go(dz(1, side, g))

    def d_step(step, *gs):
        for g in gs:
            for side in (0, 1):
                if step < nz // 2:
                    dz_in(step, side, g).wait_recv()
                    if step + 1 < nz // 2 or g in last_by[side]:
                        go(dz(step + 1, side, g))
                elif g in last_by[side]:
                    dz_in(step, side, g).wait_recv()

    def d_cores(step):
        go(d_core(step))
        if step < nz // 2:
            go(d_core(-step))

    deep = wo.shape[2]
    wo_halves = (pl.ds(0, deep // 2), pl.ds(deep // 2, deep // 2))

    def wx(step, side):
        ref = wo.at[at_x(-fwd[side] if step == 2 else 0), c].at[wo_halves[1 - side if step == 1 else side]]
        return same(ref, left_s.at[5], wo_r.at[side, step], x_to[side])

    def wx_in(step, side):
        ref = wo.at[at_x(-fwd[side] * (2 if step == 2 else 1)), c].at[wo_halves[1 - side if step == 1 else side]]
        return same(ref, left_s.at[5], wo_r.at[side, step], x_to[side])

    def w_core(i):
        return same(wo.at[at_x(i + 1), c], left_s.at[5], core_r.at[1], partner)

    def w_turn():
        for side in (0, 1):
            wx_in(0, side).wait_recv()
            go(wx(2, side))

    def w_near():
        for side in (0, 1):
            wx_in(1, side).wait_recv()
        go(w_core(0))
        go(w_core(2))

    def w_last():
        for side in (0, 1):
            wx_in(2, side).wait_recv()
        go(w_core(1))

    def w_done():
        wait_all(wo.at[pl.ds(0, nx - 1), 0], core_r.at[1])

    for load in loads[:4]:
        load.wait()

    decays[...] = jnp.zeros_like(decays)
    for b in range(blocks):
        cut = pl.ds(b * BLOCK, BLOCK)
        decays[pl.ds(3 * b, 1), :] = dw[:, cut]
        decays[pl.ds(3 * b + 1, 2), :] = dn[:, cut]
    running = decays[0:32, :]
    shift = 1
    while shift < BLOCK:
        running = running + jnp.where(lane >= shift, pltpu.roll(running, shift, 1), 0.0)
        shift *= 2
    decays[0:32, :] = running
    columns = jnp.transpose(decays[...])

    at_t = lax.broadcasted_iota(jnp.int32, (BLOCK, BLOCK), 0)
    at_s = lax.broadcasted_iota(jnp.int32, (BLOCK, BLOCK), 1)
    lower = at_t >= at_s
    same_head = (at_t < HDN) == (at_s < HDN)

    def spread(r):
        steps = jnp.minimum(columns[:, r : r + 1] - decays[pl.ds(r, 1), :], 0.0)
        return jnp.where(lower, jnp.exp(steps), 0.0)

    def angles(b):
        cos_w, sin_w = turn(base[0][0][b : b + 1], base[0][1][b : b + 1], tt[0], tt[1])
        cos_n, sin_n = turn(base[1][0][b : b + 1], base[1][1][b : b + 1], tt[2], tt[3])
        return cos_w, sin_w * sign_w, cos_n, sin_n * sign_n

    def rotate_w(a, cos, sin):
        return a * cos + pltpu.roll(a, HDW // 2, 1) * sin

    def rotate_n(a, cos, sin):
        other = jnp.where(front_n, pltpu.roll(a, 128 - HDN // 2, 1), pltpu.roll(a, HDN // 2, 1))
        return a * cos + other * sin

    def ends(b):
        r = 3 * b
        now = [columns[:, r + h : r + h + 1] for h in range(3)]
        return now, [columns[BLOCK - 1 : BLOCK, r + h : r + h + 1] for h in range(3)]

    state_w = jnp.zeros((128, 128), F32)
    state_n = jnp.zeros((128, 128), F32)
    gone = [jnp.zeros((1, 1), F32)] * 3
    before_block = []
    for b in range(blocks):
        cut = pl.ds(b * BLOCK, BLOCK)
        now, last = ends(b)
        cos_w, sin_w, cos_n, sin_n = angles(b)
        st_w[b] = state_w.astype(BF16)
        st_n[b] = state_n.astype(BF16)
        before_block.append(gone)
        k = rotate_w(kw[cut, :].astype(F32), cos_w, sin_w) * HDW**-0.5
        k_w[cut, :] = k.astype(BF16)
        tail = k * jnp.exp(last[0] - now[0])
        state_w = jnp.exp(last[0]) * state_w + tdot(tail.astype(BF16), vw[cut, :])
        k = rotate_n(kn[cut, :].astype(F32), cos_n, sin_n) * HDN**-0.5
        k_n[cut, :] = k.astype(BF16)
        tail = k * jnp.where(low, jnp.exp(last[1] - now[1]), jnp.exp(last[2] - now[2]))
        keep = jnp.where(low, jnp.exp(last[1]), jnp.exp(last[2]))
        state_n = keep * state_n + jnp.where(same_head, tdot(tail.astype(BF16), vn[cut, :]), 0.0)
        gone = [g + t for g, t in zip(gone, last)]

    def outputs(b):
        cut = pl.ds(b * BLOCK, BLOCK)
        r = 3 * b
        now, last = ends(b)
        cos_w, sin_w, cos_n, sin_n = angles(b)
        gone = before_block[b]
        q = rotate_w(qw[cut, :].astype(F32), cos_w, sin_w)
        scores = dot_t(q.astype(BF16), k_w[cut, :]) * spread(r)
        out_b = dot(scores.astype(BF16), vw[cut, :])
        if b:
            out_b += dot((q * jnp.exp(now[0])).astype(BF16), st_w[b])
        o_w[cut, :] = out_b
        qe_w[cut, :] = (q * jnp.exp(now[0] + gone[0])).astype(BF16)
        q = rotate_n(qn[cut, :].astype(F32), cos_n, sin_n)
        probs = []
        for h, mask in enumerate((low, jnp.logical_not(low))):
            qh = jnp.where(mask, q, 0.0).astype(BF16)
            probs.append((dot_t(qh, k_n[cut, :]) * spread(r + 1 + h)).astype(BF16))
        v_f = vn[cut, :].astype(F32)
        v2 = jnp.concatenate(
            [jnp.where(low, v_f, 0.0).astype(BF16), jnp.where(low, 0.0, v_f).astype(BF16)], axis=0
        )
        out_b = dot(jnp.concatenate(probs, axis=1), v2)
        if b:
            seen = jnp.where(low, jnp.exp(now[1]), jnp.exp(now[2]))
            out_b += dot((q * seen).astype(BF16), st_n[b])
        o_n[cut, :] = out_b
        seen = jnp.where(low, jnp.exp(now[1] + gone[1]), jnp.exp(now[2] + gone[2]))
        qe_n[cut, :] = (q * seen).astype(BF16)

    total_w = jnp.exp(gone[0]) + jnp.zeros((1, 128), F32)
    total_n = jnp.where(low, jnp.exp(gone[1]), jnp.exp(gone[2]))
    packed_n = jnp.where(low, state_n[:HDN], state_n[HDN:])
    sw, sn = 128 // plane, HDN // plane
    part_of = lax.broadcasted_iota(jnp.int32, (8, 128), 0)

    def message(state, rate_w, rate_n):
        parts = jnp.zeros((8, 128), F32)
        for r, rate in ((0, rate_w), (2, rate_n)):
            high = rate.astype(BF16).astype(F32)
            parts = jnp.where(part_of == r, high, jnp.where(part_of == r + 1, rate - high, parts))
        return jnp.concatenate([state, parts], axis=0).astype(BF16)

    for j in range(plane):
        state = [state_w[sw * j : sw * (j + 1)], packed_n[sn * j : sn * (j + 1)]]
        msg[j] = message(jnp.concatenate(state, axis=0), total_w, total_n)
    ns = sw + sn

    def stage1(d):
        to = lax.rem(me + d, plane)
        return remote(msg.at[to], in1.at[me], left_s.at[10], s1_r, at_plane(to))

    pl.semaphore_wait(barrier, len(peers))
    for d in range(1, plane):
        stage1(d).start()
    for load in loads[4:10]:
        load.wait()
    for side in (0, 1):
        go(uz(1, side))
        go(wx(0, side))
    d_own()
    for side in (0, 1):
        go(wx(1, side))
    in1[pl.ds(me, 1)] = msg[pl.ds(me, 1)]
    for b in range(blocks // 2):
        outputs(b)

    wait_all(msg.at[pl.ds(0, plane - 1)], s1_r)
    wide_row = lax.broadcasted_iota(jnp.int32, (ns, 128), 0) < sw

    def factor(pair):
        return jnp.where(wide_row, pair[0], pair[1])

    def opened(ref, j):
        whole = ref[j].astype(F32)
        return whole[0:ns], (whole[ns : ns + 1] + whole[ns + 1 : ns + 2], whole[ns + 2 : ns + 3] + whole[ns + 3 : ns + 4])

    before = []
    held = jnp.zeros((ns, 128), F32)
    rate = (jnp.ones((1, 128), F32), jnp.ones((1, 128), F32))
    for j in range(plane):
        before.append((held, rate))
        state, mine = opened(in1, j)
        held = held * factor(mine) + state
        rate = (rate[0] * mine[0], rate[1] * mine[1])
    tot2[...] = message(held, *rate)

    def stage2(d):
        return remote(tot2, in2.at[z], left_s.at[11], s2_r, {"z": lax.rem(z + d, nz)})

    for d in range(1, nz):
        stage2(d).start()
    for side in (0, 1):
        go(uy(0, side))
    d_send(0)
    for b in range(blocks // 2, blocks):
        outputs(b)
    u_step(1)
    d_turn()
    d_send(1)
    w_turn()
    in2[pl.ds(z, 1)] = tot2[...][None]
    wait_all(in2.at[pl.ds(0, nz - 1)], s2_r)
    held = jnp.zeros((ns, 128), F32)
    for k in range(nz):
        state, mine = opened(in2, k)
        later = held * factor(mine) + state
        held = jnp.where(k < z, later, held)
    for j in range(plane):
        state, rate = before[j]
        state = held * factor(rate) + state
        msg3[j] = jnp.concatenate([state, jnp.zeros((8, 128), F32)], axis=0).astype(BF16)

    def stage3(d):
        to = lax.rem(me + d, plane)
        return remote(msg3.at[to], in3.at[me], left_s.at[12], s3_r, at_plane(to))

    for d in range(1, plane):
        stage3(d).start()
    in3[pl.ds(me, 1)] = msg3[pl.ds(me, 1)]
    u_turn(1)
    u_relay((0, 0))
    d_column()
    w_near()
    u_step(2)
    u_turn(2)
    d_send(2)
    for load in loads[10:]:
        load.wait()
    wait_all(msg.at[pl.ds(0, plane - 1)], s3_r)
    arrived = in3[...].astype(F32)
    enter_w = arrived[:, 0:sw, :].reshape(128, 128).astype(BF16)
    enter_p = arrived[:, sw:ns, :].reshape(HDN, 128)
    enter_n = jnp.concatenate(
        [jnp.where(low, enter_p, 0.0), jnp.where(low, 0.0, enter_p)], axis=0
    ).astype(BF16)

    def mixed_to(d):
        to = lax.rem(x + d, nx)
        return remote(mixed.at[to], mix_in.at[x], left_s.at[7], mx_r, {"x": to})

    def gated(o, gate):
        return (o * jax.nn.silu(gate.astype(F32))).astype(BF16)

    for d in (2, 1, 3, 0):
        i = lax.rem(x + d, nx)
        cut = pl.ds(pl.multiple_of(i * rows, rows), rows)
        o = o_w[cut, :] + dot(qe_w[cut, :], enter_w)
        o = o - jnp.mean(o, axis=-1, keepdims=True)
        o = o * lax.rsqrt(jnp.mean(o * o, axis=-1, keepdims=True) + head_eps)
        mixed[i, :, 0:128] = gated(o, gw[cut, :])
        o = o_n[cut, :] + dot(qe_n[cut, :], enter_n)

        def by_head(a):
            first = jnp.sum(jnp.where(low, a, 0.0), axis=-1, keepdims=True)
            second = jnp.sum(jnp.where(low, 0.0, a), axis=-1, keepdims=True)
            return jnp.where(low, first, second) * (1.0 / HDN)

        o = o - by_head(o)
        o = o * lax.rsqrt(by_head(o * o) + head_eps)
        mixed[i, :, 128:256] = gated(o, gn[cut, :])
        if d:
            go(mixed_to(d))

    mix_in[pl.ds(x, 1)] = mixed[pl.ds(x, 1)]

    u_relay((1, 1))
    w_last()
    u_step(3)
    u_turn(3)
    d_send(3)
    d_step(1, 0, 1)
    u_relay((1, 0))
    w_done()
    wait_all(mixed.at[pl.ds(0, nx - 1)], mx_r)

    tile = 512
    tiles = width // tile

    def project(n, squares):
        at = pl.ds(pl.multiple_of(n * tile, tile), tile)
        total = stream[:, at].astype(F32)
        for j in range(nx):
            total += dot(mix_in[j], wo[j, :, :, at].reshape(2 * deep, tile))
        total = total.astype(BF16)
        middle[:, at] = total
        total = total.astype(F32)
        return squares + jnp.sum(total * total, axis=-1, keepdims=True)

    squares = lax.fori_loop(0, tiles, project, jnp.zeros((rows, 1), F32))
    scale = lax.rsqrt(squares * (1.0 / width) + norm_eps)
    normed[pl.ds(x, 1)] = (middle[...].astype(F32) * scale * gain[...].astype(F32).reshape(1, width)).astype(BF16)[None]

    def nx_rows(piece, side):
        if piece in (0, 3):
            return pl.ds(side * half_rows, half_rows)
        start = (1 - side) * half_rows
        return pl.ds(start, few) if piece == 1 else pl.ds(start + few, half_rows - few)

    def nm(piece, side):
        ref = normed.at[at_x(-fwd[side] if piece == 3 else 0), nx_rows(piece, side)]
        return same(ref, left_s.at[8], st_r.at[side, piece], x_to[side])

    def nm_in(piece, side):
        ref = normed.at[at_x(-fwd[side] * (2 if piece == 3 else 1)), nx_rows(piece, side)]
        return same(ref, left_s.at[8], st_r.at[side, piece], x_to[side])

    for piece in (0, 1):
        for side in (0, 1):
            go(nm(piece, side))

    u_relay((2, 1))
    d_step(1, 2)
    u_step(4)
    u_turn(4)
    d_step(1, 3)
    d_cores(1)
    u_relay((2, 0))
    d_step(2, 0)
    u_relay((3, 1))
    d_step(2, 1)
    u_relay((3, 0))
    d_step(2, 2)
    for side in (0, 1):
        nm_in(0, side).wait_recv()
        go(nm(3, side))
        go(nm(2, side))
    u_relay((0, 1))
    d_step(2, 3)
    d_cores(2)
    u_rest()
    d_step(3, 0, 1)
    u_last()
    d_step(3, 2)
    u_done()

    def rise(i):
        def one(n, _):
            at = pl.ds(pl.multiple_of(n * tile, tile), tile)
            h = jnp.maximum(dot(normed[i], up[:, :, :, :, at].reshape(width, tile)), 0.0)
            hidden[i, :, at] = (h * h).astype(BF16)
            return 0

        lax.fori_loop(0, tiles, one, 0)

    for side in (0, 1):
        nm_in(3, side).wait_recv()
    rise(xo)
    d_step(3, 3)
    d_cores(3)

    span = width // nz
    blocks_of = (by_distance[:early], by_distance[early:])
    lanes_of = (pl.ds(0, early * span), pl.ds(early * span, width - early * span))

    first, second = slice(0, half_rows), slice(half_rows, rows)

    def fall(i, half, put):
        for n, k in enumerate(blocks_of[half]):
            at = (half * early + n) * span
            put(slice(at, at + span), dot_t(hidden[i], down[at_z(k)].reshape(span, width)))

    def put_far(at, piece):
        send2[:, at] = piece.astype(BF16)

    def put_right(at, piece):
        send1[second, at] = piece[second].astype(BF16)
        hold[0, :, at] = piece[first]

    def put_left(at, piece):
        sendm[first, at] = piece[first].astype(BF16)
        hold[1, :, at] = piece[second]

    def put_own(at, piece):
        own[:, at] = piece

    got_l, got_r = got_both.at[0], got_both.at[1]
    row_halves = (pl.ds(0, half_rows), pl.ds(half_rows, half_rows))

    def far(half, side):
        to = (relay_l, relay_r)[side].at[:, lanes_of[half]]
        return remote(send2.at[row_halves[side], lanes_of[half]], to, left_s.at[9], rs_r.at[2 * half + side], x_to[side])

    def near(half, side, summed):
        at = (row_halves[side if summed else 1 - side], lanes_of[half])
        source, to = ((send1, got_l), (sendm, got_r))[side]
        return remote(source.at[at], to.at[at], left_s.at[9], rs_r.at[4 + half], x_to[side])

    def add_far(half):
        at = lanes_of[half]
        far(half, 0).wait_recv()
        send1[first, at] = (hold[0, :, at] + relay_l[:, at].astype(F32)).astype(BF16)
        go(near(half, 0, 1))
        far(half, 1).wait_recv()
        sendm[second, at] = (hold[1, :, at] + relay_r[:, at].astype(F32)).astype(BF16)
        go(near(half, 1, 1))

    wait_all(down.at[pl.ds(0, early), :, 0], core_r.at[2])
    fall(xo, 0, put_far)
    for side in (0, 1):
        go(far(0, side))
    for side in (0, 1):
        for piece in (1, 2):
            nm_in(piece, side).wait_recv()
    rise(xl)
    d_step(4, 0, 1, 2, 3)
    d_cores(4)
    fall(xl, 0, put_left)
    go(near(0, 1, 0))
    wait_all(down.at[pl.ds(0, nz - early), :, 0], core_r.at[3])
    fall(xo, 1, put_far)
    for side in (0, 1):
        go(far(1, side))
    rise(xr)
    fall(xr, 0, put_right)
    go(near(0, 0, 0))
    add_far(0)
    fall(xr, 1, put_right)
    go(near(1, 0, 0))
    fall(xl, 1, put_left)
    go(near(1, 1, 0))
    add_far(1)
    rise(x)
    fall(x, 0, put_own)
    fall(x, 1, put_own)
    for half in (0, 1):
        at = lanes_of[half]
        wait_all(got_both.at[:, :, at], rs_r.at[4 + half])
        total = own[:, at] + got_l[:, at].astype(F32) + got_r[:, at].astype(F32)
        for n, k in enumerate(blocks_of[half]):
            at = pl.ds(pl.multiple_of(at_z(k) * span, span), span)
            result[:, at] = (middle[:, at].astype(F32) + total[:, n * span : (n + 1) * span]).astype(BF16)
            go(pltpu.make_async_copy(result.at[:, at], out.at[:, at], out_s))

    totals = (
        up.at[pl.ds(0, nz - 1), 0, 0], up.at[:, pl.ds(0, 2), 0], up.at[:, 0, 0], down.at[pl.ds(0, 3), 0, 0],
        down.at[pl.ds(0, nz - 1), :, 0], wo.at[pl.ds(0, 3)], up, mixed.at[pl.ds(0, nx - 1)], normed.at[pl.ds(0, 3)],
        normed.at[pl.ds(0, 3)], msg.at[pl.ds(0, plane - 1)], in2.at[pl.ds(0, nz - 1)], msg.at[pl.ds(0, plane - 1)],
    )
    for i, total in enumerate(totals):
        wait_all(total, left_s.at[i])
    wait_all(out, out_s)


def on_device(
    sizes,
    stream_in, query_wide, key_wide, value_wide, gate_wide, decay_wide,
    query_narrow, key_narrow, value_narrow, gate_narrow, decay_narrow,
    output_wide, output_narrow, norm_gain, up_weight, down_weight,
):
    nz, ny, nc, nx = sizes
    tok = query_wide.shape[0]
    rows, width = stream_in.shape
    plane = ny * nc
    part, hid = up_weight.shape
    ns = (128 + HDN) // plane
    dma = pltpu.SemaphoreType.DMA
    vm = pltpu.VMEM
    scratch = [
        *[vm((tok, 128), BF16)] * 8, vm((rows, width), BF16),
        vm((nz, ny, nc, part, hid), BF16), vm((nz, ny, nc, part, hid), BF16), vm((nx, 2, *output_wide.shape), BF16),
        vm((tok, 128), BF16), vm((tok, 128), BF16), vm((tok, 128), F32), vm((tok, 128), F32),
        vm((128, 128), F32),
        vm((tok // BLOCK, 128, 128), BF16), vm((tok // BLOCK, 128, 128), BF16), vm((tok, 128), BF16), vm((tok, 128), BF16),
        vm((plane, ns + 8, 128), BF16), vm((plane, ns + 8, 128), BF16),
        vm((ns + 8, 128), BF16), vm((nz, ns + 8, 128), BF16),
        vm((plane, ns + 8, 128), BF16), vm((plane, ns + 8, 128), BF16),
        vm((nx, rows, 256), BF16), vm((nx, rows, 256), BF16),
        vm((rows, width), BF16), vm((nx, rows, width), BF16), vm((nx, rows, hid), BF16),
        vm((rows, width), BF16), vm((rows, width), BF16), vm((rows, width), BF16),
        vm((rows, width), F32), vm((2, rows // 2, width), F32), vm((rows, width), BF16),
        vm((rows // 2, width), BF16), vm((rows // 2, width), BF16), vm((2, rows, width), BF16),
        dma((13,)), dma((13,)), dma, dma((2, 4)), dma, dma, dma, dma, dma((6,)), dma((2, 3)), dma((2, 4)), dma((2, 5)),
        dma, dma((2, 2)), dma((2, 4, 4)), dma((4,)),
    ]
    vmem = pl.BlockSpec(memory_space=pltpu.VMEM)
    hbm = pl.BlockSpec(memory_space=pl.ANY)
    return pl.pallas_call(
        functools.partial(kernel, sizes),
        out_shape=jax.ShapeDtypeStruct((rows, width), BF16),
        in_specs=[vmem] * 6 + [hbm] * 13,
        out_specs=hbm,
        scratch_shapes=scratch,
        compiler_params=pltpu.CompilerParams(
            collective_id=0, has_side_effects=True, vmem_limit_bytes=60 * 1024 * 1024
        ),
    )(
        decay_wide, decay_narrow, norm_gain, jnp.asarray(rope_tables(BLOCK, 1)),
        jnp.asarray(rope_tables(8, BLOCK)), jnp.asarray(rope_tables(nz * plane, tok)),
        query_wide, key_wide, value_wide, query_narrow, key_narrow, value_narrow, gate_wide, gate_narrow, stream_in,
        output_wide, output_narrow, up_weight, down_weight.T,
    )


def solution(mesh):
    sizes = (8, 4, 2, mesh.shape["tp"])
    split = Mesh(mesh.devices.reshape(sizes), ("z", "y", "c", "x"))
    sp = ("z", "y", "c")
    rows, heads = P(sp, "x"), P("x", sp)
    in_specs = (
        P((*sp, "x"), None), rows, rows, rows, rows, heads, rows, rows, rows, rows, heads,
        P("x", None), P("x", None), P(), rows, heads,
    )
    return jax.shard_map(
        functools.partial(on_device, sizes), mesh=split, in_specs=in_specs,
        out_specs=P((*sp, "x"), None), check_vma=False,
    )
```

time: 102 us -> 96.7 us (0.948)
  Pallas kernels: 99.4 us -> 94.4 us
    pallas_call x1, Pallas kernels: 99.4 us -> 94.4 us  [on_device(): pl.pallas_call(functools.partial(kernel, sizes), out_shape=jax.ShapeDtype...]
where the time goes in v4:
time: 96.7 us; the launch traced here: 96.5 us
  Pallas kernels  94.4 us (98%)
  local copies, waits for them, and re-layouts  2.09 us (2%)
    pallas_call x1, Pallas kernels, on_device(): pl.pallas_call(functools.partial(kernel, sizes), out_shape=jax.ShapeDtype...  94.4 us
    unnamed x1, local copies, waits for them, and re-layouts  2.09 us

profile of v4, /device:TPU:1, one launch (start us, length us, event | category | flops | bytes accessed | tf_op | source)
XLA Modules:
  0.0 96.5 jit_solution(4744103354736971959)
XLA Ops:
  0.0 94.4 %shard_map.181 = bf16[192,2048]{1,0:T(8,128)(2,1)} custom-call(f32[1,768]{1,0:T(1,128)} %dw.1, f32[2,768]{1,0:T(2,128)} %dn.1, bf16[2048]{0:T(1024)(128)(2,1)} %gain.1, f32[4,128,128]{2,1,0:T(8,128)} %constant.6.clone.tt, f32[4,8,128]{2,1,0:T(8,128)} %constant.7.clone.tb, f32[4,64,128]{2,1,0:T(8,128)} %constant.8.clone.ts, bf16[768,128]{1,0:T(8,128)(2,1)} %qw_in.1, ...), custom_call_target="tpu_custom_call" | custom-call | tf_op jit(solution)/shard_map/pallas_call | solution.py:735
  94.4 2.1 %copy.21 = bf16[192,2048]{1,0:T(8,128)(2,1)} copy(bf16[192,2048]{1,0:T(8,128)(2,1)} %shard_map.181) | data formatting | bytes 1572864

commit v5 on v4

--- a/solution.py
+++ b/solution.py
@@ -74,7 +74,7 @@
     blocks = tok // BLOCK
     rows = stream.shape[0]
     width = stream.shape[1]
-    half_rows, few = rows // 2, rows // 6
+    half_rows, part_rows = rows // 2, rows // 4
     right, left = {"x": xr}, {"x": xl}
 
     def at_plane(j):
@@ -549,18 +549,22 @@
     normed[pl.ds(x, 1)] = (middle[...].astype(F32) * scale * gain[...].astype(F32).reshape(1, width)).astype(BF16)[None]
 
     def nx_rows(piece, side):
-        if piece in (0, 3):
-            return pl.ds(side * half_rows, half_rows)
-        start = (1 - side) * half_rows
-        return pl.ds(start, few) if piece == 1 else pl.ds(start + few, half_rows - few)
+        if piece == 4:
+            return pl.ds((1 - side) * half_rows, half_rows)
+        return pl.ds(side * half_rows + piece % 2 * part_rows, part_rows)
 
     def nm(piece, side):
-        ref = normed.at[at_x(-fwd[side] if piece == 3 else 0), nx_rows(piece, side)]
+        ref = normed.at[at_x(-fwd[side] if piece in (2, 3) else 0), nx_rows(piece, side)]
         return same(ref, left_s.at[8], st_r.at[side, piece], x_to[side])
 
     def nm_in(piece, side):
-        ref = normed.at[at_x(-fwd[side] * (2 if piece == 3 else 1)), nx_rows(piece, side)]
+        ref = normed.at[at_x(-fwd[side] * (2 if piece in (2, 3) else 1)), nx_rows(piece, side)]
         return same(ref, left_s.at[8], st_r.at[side, piece], x_to[side])
+
+    def nm_on(piece):
+        for side in (0, 1):
+            nm_in(piece, side).wait_recv()
+            go(nm(piece + 2, side))
 
     for piece in (0, 1):
         for side in (0, 1):
@@ -576,35 +580,37 @@
     d_step(2, 0)
     u_relay((3, 1))
     d_step(2, 1)
+    nm_on(0)
     u_relay((3, 0))
     d_step(2, 2)
-    for side in (0, 1):
-        nm_in(0, side).wait_recv()
-        go(nm(3, side))
-        go(nm(2, side))
+    nm_on(1)
+    for side in (0, 1):
+        go(nm(4, side))
     u_relay((0, 1))
     d_step(2, 3)
     d_cores(2)
     u_rest()
-    d_step(3, 0, 1)
+    d_step(3, 0)
     u_last()
-    d_step(3, 2)
+    d_step(3, 1)
     u_done()
 
-    def rise(i):
+    near_rows = ((xl, 0, xr, 1), (xo, 0, xo, 1), (xr, 0, xl, 1), (x, 0, x, 1))
+    EARLY, FAR, LATE, OWN = range(4)
+
+    def rise(batch):
+        slot_a, half_a, slot_b, half_b = near_rows[batch]
+
         def one(n, _):
             at = pl.ds(pl.multiple_of(n * tile, tile), tile)
-            h = jnp.maximum(dot(normed[i], up[:, :, :, :, at].reshape(width, tile)), 0.0)
-            hidden[i, :, at] = (h * h).astype(BF16)
+            a = normed[slot_a, half_a * half_rows : (half_a + 1) * half_rows]
+            b = normed[slot_b, half_b * half_rows : (half_b + 1) * half_rows]
+            h = dot(jnp.concatenate([a, b], axis=0), up[:, :, :, :, at].reshape(width, tile))
+            h = jnp.maximum(h, 0.0)
+            hidden[batch, :, at] = (h * h).astype(BF16)
             return 0
 
         lax.fori_loop(0, tiles, one, 0)
-
-    for side in (0, 1):
-        nm_in(3, side).wait_recv()
-    rise(xo)
-    d_step(3, 3)
-    d_cores(3)
 
     span = width // nz
     blocks_of = (by_distance[:early], by_distance[early:])
@@ -612,20 +618,20 @@
 
     first, second = slice(0, half_rows), slice(half_rows, rows)
 
-    def fall(i, half, put):
+    def fall(batch, half, put):
         for n, k in enumerate(blocks_of[half]):
             at = (half * early + n) * span
-            put(slice(at, at + span), dot_t(hidden[i], down[at_z(k)].reshape(span, width)))
+            put(slice(at, at + span), dot_t(hidden[batch], down[at_z(k)].reshape(span, width)))
 
     def put_far(at, piece):
         send2[:, at] = piece.astype(BF16)
 
-    def put_right(at, piece):
+    def put_early(at, piece):
+        sendm[first, at] = piece[first].astype(BF16)
         send1[second, at] = piece[second].astype(BF16)
+
+    def put_late(at, piece):
         hold[0, :, at] = piece[first]
-
-    def put_left(at, piece):
-        sendm[first, at] = piece[first].astype(BF16)
         hold[1, :, at] = piece[second]
 
     def put_own(at, piece):
@@ -652,34 +658,40 @@
         sendm[second, at] = (hold[1, :, at] + relay_r[:, at].astype(F32)).astype(BF16)
         go(near(half, 1, 1))
 
+    rise(EARLY)
+    d_step(3, 2)
     wait_all(down.at[pl.ds(0, early), :, 0], core_r.at[2])
-    fall(xo, 0, put_far)
+    fall(EARLY, 0, put_early)
+    for side in (0, 1):
+        go(near(0, side, 0))
+    for side in (0, 1):
+        nm_in(2, side).wait_recv()
+        nm_in(3, side).wait_recv()
+    d_step(3, 3)
+    d_cores(3)
+    rise(FAR)
+    fall(FAR, 0, put_far)
     for side in (0, 1):
         go(far(0, side))
-    for side in (0, 1):
-        for piece in (1, 2):
-            nm_in(piece, side).wait_recv()
-    rise(xl)
     d_step(4, 0, 1, 2, 3)
     d_cores(4)
-    fall(xl, 0, put_left)
-    go(near(0, 1, 0))
+    for side in (0, 1):
+        nm_in(4, side).wait_recv()
+    rise(LATE)
+    fall(LATE, 0, put_late)
     wait_all(down.at[pl.ds(0, nz - early), :, 0], core_r.at[3])
-    fall(xo, 1, put_far)
+    fall(EARLY, 1, put_early)
+    for side in (0, 1):
+        go(near(1, side, 0))
+    fall(FAR, 1, put_far)
     for side in (0, 1):
         go(far(1, side))
-    rise(xr)
-    fall(xr, 0, put_right)
-    go(near(0, 0, 0))
     add_far(0)
-    fall(xr, 1, put_right)
-    go(near(1, 0, 0))
-    fall(xl, 1, put_left)
-    go(near(1, 1, 0))
+    fall(LATE, 1, put_late)
     add_far(1)
-    rise(x)
-    fall(x, 0, put_own)
-    fall(x, 1, put_own)
+    rise(OWN)
+    fall(OWN, 0, put_own)
+    fall(OWN, 1, put_own)
     for half in (0, 1):
         at = lanes_of[half]
         wait_all(got_both.at[:, :, at], rs_r.at[4 + half])
@@ -727,7 +739,7 @@
         vm((rows, width), BF16), vm((rows, width), BF16), vm((rows, width), BF16),
         vm((rows, width), F32), vm((2, rows // 2, width), F32), vm((rows, width), BF16),
         vm((rows // 2, width), BF16), vm((rows // 2, width), BF16), vm((2, rows, width), BF16),
-        dma((13,)), dma((13,)), dma, dma((2, 4)), dma, dma, dma, dma, dma((6,)), dma((2, 3)), dma((2, 4)), dma((2, 5)),
+        dma((13,)), dma((13,)), dma, dma((2, 5)), dma, dma, dma, dma, dma((6,)), dma((2, 3)), dma((2, 4)), dma((2, 5)),
         dma, dma((2, 2)), dma((2, 4, 4)), dma((4,)),
     ]
     vmem = pl.BlockSpec(memory_space=pltpu.VMEM)

time: 96.7 us -> 93.2 us (0.964)
  Pallas kernels: 94.4 us -> 91 us
    pallas_call x1, Pallas kernels: 94.4 us -> 91 us  [on_device(): pl.pallas_call(functools.partial(kernel, sizes), out_shape=jax.ShapeDtype...]
where the time goes in v5:
time: 93.2 us; the launch traced here: 93.1 us
  Pallas kernels  91 us (98%)
  local copies, waits for them, and re-layouts  2.09 us (2%)
    pallas_call x1, Pallas kernels, on_device(): pl.pallas_call(functools.partial(kernel, sizes), out_shape=jax.ShapeDtype...  91 us
    unnamed x1, local copies, waits for them, and re-layouts  2.09 us

profile of v5, /device:TPU:1, one launch (start us, length us, event | category | flops | bytes accessed | tf_op | source)
XLA Modules:
  0.0 93.1 jit_solution(6543051475082480298)
XLA Ops:
  0.0 91.0 %shard_map.181 = bf16[192,2048]{1,0:T(8,128)(2,1)} custom-call(f32[1,768]{1,0:T(1,128)} %dw.1, f32[2,768]{1,0:T(2,128)} %dn.1, bf16[2048]{0:T(1024)(128)(2,1)} %gain.1, f32[4,128,128]{2,1,0:T(8,128)} %constant.6.clone.tt, f32[4,8,128]{2,1,0:T(8,128)} %constant.7.clone.tb, f32[4,64,128]{2,1,0:T(8,128)} %constant.8.clone.ts, bf16[768,128]{1,0:T(8,128)(2,1)} %qw_in.1, ...), custom_call_target="tpu_custom_call" | custom-call | tf_op jit(solution)/shard_map/pallas_call | solution.py:747
  91.0 2.1 %copy.21 = bf16[192,2048]{1,0:T(8,128)(2,1)} copy(bf16[192,2048]{1,0:T(8,128)(2,1)} %shard_map.181) | data formatting | bytes 1572864

commit v6 on v5

--- a/solution.py
+++ b/solution.py
@@ -155,9 +155,11 @@
         return same(ref, left_s.at[1], uy_r.at[side, relayed[side].index(off) if off in relayed[side] else 4], y_to[side])
 
 
+    relays = (((0, 0), (1, 1), (1, 0), (2, 1)), ((2, 0), (3, 1), (3, 0), (0, 1)))
+
     def ur(i, side):
         ref = up.at[at_z(relayed[side][i]), at_y(-fwd[side]), c]
-        return same(ref, left_s.at[2], ur_r, y_to[side])
+        return same(ref, left_s.at[2], ur_r.at[0 if (i, side) in relays[0] else 1], y_to[side])
 
     def u_core(i):
         ref = up.at[:, at_y((0, 1, -1, 2)[i]), c]
@@ -188,9 +190,10 @@
         go(u_core(1))
         go(u_core(2))
 
-    def u_last():
-        wait_all(up.at[:, 0, 0], ur_r)
-        go(u_core(3))
+    def u_last(group):
+        wait_all(up.at[pl.ds(0, 4), 0, 0], ur_r.at[group])
+        for i, side in relays[group]:
+            go(same(up.at[at_z(relayed[side][i]), at_y(2), c], left_s.at[6], core_r.at[0], partner))
 
     def u_done():
         wait_all(up.at[:, :, 0], core_r.at[0])
@@ -478,10 +481,10 @@
     u_turn(1)
     u_relay((0, 0))
     d_column()
-    w_near()
     u_step(2)
     u_turn(2)
     d_send(2)
+    w_near()
     for load in loads[10:]:
         load.wait()
     wait_all(msg.at[pl.ds(0, plane - 1)], s3_r)
@@ -522,12 +525,12 @@
     mix_in[pl.ds(x, 1)] = mixed[pl.ds(x, 1)]
 
     u_relay((1, 1))
-    w_last()
     u_step(3)
     u_turn(3)
     d_send(3)
     d_step(1, 0, 1)
     u_relay((1, 0))
+    w_last()
     w_done()
     wait_all(mixed.at[pl.ds(0, nx - 1)], mx_r)
 
@@ -570,10 +573,10 @@
         for side in (0, 1):
             go(nm(piece, side))
 
+    u_step(4)
+    u_turn(4)
     u_relay((2, 1))
     d_step(1, 2)
-    u_step(4)
-    u_turn(4)
     d_step(1, 3)
     d_cores(1)
     u_relay((2, 0))
@@ -584,6 +587,7 @@
     u_relay((3, 0))
     d_step(2, 2)
     nm_on(1)
+    u_last(0)
     for side in (0, 1):
         go(nm(4, side))
     u_relay((0, 1))
@@ -591,7 +595,7 @@
     d_cores(2)
     u_rest()
     d_step(3, 0)
-    u_last()
+    u_last(1)
     d_step(3, 1)
     u_done()
 
@@ -688,8 +692,8 @@
         go(far(1, side))
     add_far(0)
     fall(LATE, 1, put_late)
+    rise(OWN)
     add_far(1)
-    rise(OWN)
     fall(OWN, 0, put_own)
     fall(OWN, 1, put_own)
     for half in (0, 1):
@@ -740,7 +744,7 @@
         vm((rows, width), F32), vm((2, rows // 2, width), F32), vm((rows, width), BF16),
         vm((rows // 2, width), BF16), vm((rows // 2, width), BF16), vm((2, rows, width), BF16),
         dma((13,)), dma((13,)), dma, dma((2, 5)), dma, dma, dma, dma, dma((6,)), dma((2, 3)), dma((2, 4)), dma((2, 5)),
-        dma, dma((2, 2)), dma((2, 4, 4)), dma((4,)),
+        dma((2,)), dma((2, 2)), dma((2, 4, 4)), dma((4,)),
     ]
     vmem = pl.BlockSpec(memory_space=pltpu.VMEM)
     hbm = pl.BlockSpec(memory_space=pl.ANY)

time: 93.2 us -> 91.8 us (0.985)
  Pallas kernels: 91 us -> 89.5 us
    pallas_call x1, Pallas kernels: 91 us -> 89.5 us  [on_device(): pl.pallas_call(functools.partial(kernel, sizes), out_shape=jax.ShapeDtype...]
where the time goes in v6:
time: 91.8 us; the launch traced here: 91.6 us
  Pallas kernels  89.5 us (97%)
  local copies, waits for them, and re-layouts  2.09 us (2%)
    pallas_call x1, Pallas kernels, on_device(): pl.pallas_call(functools.partial(kernel, sizes), out_shape=jax.ShapeDtype...  89.5 us
    unnamed x1, local copies, waits for them, and re-layouts  2.09 us

profile of v6, /device:TPU:1, one launch (start us, length us, event | category | flops | bytes accessed | tf_op | source)
XLA Modules:
  0.0 91.6 jit_solution(13990891643251761324)
XLA Ops:
  0.0 89.5 %shard_map.181 = bf16[192,2048]{1,0:T(8,128)(2,1)} custom-call(f32[1,768]{1,0:T(1,128)} %dw.1, f32[2,768]{1,0:T(2,128)} %dn.1, bf16[2048]{0:T(1024)(128)(2,1)} %gain.1, f32[4,128,128]{2,1,0:T(8,128)} %constant.6.clone.tt, f32[4,8,128]{2,1,0:T(8,128)} %constant.7.clone.tb, f32[4,64,128]{2,1,0:T(8,128)} %constant.8.clone.ts, bf16[768,128]{1,0:T(8,128)(2,1)} %qw_in.1, ...), custom_call_target="tpu_custom_call" | custom-call | tf_op jit(solution)/shard_map/pallas_call | solution.py:751
  89.5 2.1 %copy.21 = bf16[192,2048]{1,0:T(8,128)(2,1)} copy(bf16[192,2048]{1,0:T(8,128)(2,1)} %shard_map.181) | data formatting | bytes 1572864

commit v7 on v6

--- a/solution.py
+++ b/solution.py
@@ -690,11 +690,11 @@
     fall(FAR, 1, put_far)
     for side in (0, 1):
         go(far(1, side))
+    fall(LATE, 1, put_late)
     add_far(0)
-    fall(LATE, 1, put_late)
     rise(OWN)
+    fall(OWN, 0, put_own)
     add_far(1)
-    fall(OWN, 0, put_own)
     fall(OWN, 1, put_own)
     for half in (0, 1):
         at = lanes_of[half]

time: 91.8 us -> 91.8 us (level)
  no operation moved by 1% of the time
where the time goes in v7:
time: 91.8 us; the launch traced here: 91.6 us
  Pallas kernels  89.5 us (97%)
  local copies, waits for them, and re-layouts  2.09 us (2%)
    pallas_call x1, Pallas kernels, on_device(): pl.pallas_call(functools.partial(kernel, sizes), out_shape=jax.ShapeDtype...  89.5 us
    unnamed x1, local copies, waits for them, and re-layouts  2.09 us

profile of v7, /device:TPU:1, one launch (start us, length us, event | category | flops | bytes accessed | tf_op | source)
XLA Modules:
  0.0 91.6 jit_solution(15477088136275976663)
XLA Ops:
  0.0 89.5 %shard_map.181 = bf16[192,2048]{1,0:T(8,128)(2,1)} custom-call(f32[1,768]{1,0:T(1,128)} %dw.1, f32[2,768]{1,0:T(2,128)} %dn.1, bf16[2048]{0:T(1024)(128)(2,1)} %gain.1, f32[4,128,128]{2,1,0:T(8,128)} %constant.6.clone.tt, f32[4,8,128]{2,1,0:T(8,128)} %constant.7.clone.tb, f32[4,64,128]{2,1,0:T(8,128)} %constant.8.clone.ts, bf16[768,128]{1,0:T(8,128)(2,1)} %qw_in.1, ...), custom_call_target="tpu_custom_call" | custom-call | tf_op jit(solution)/shard_map/pallas_call | solution.py:751
  89.5 2.1 %copy.21 = bf16[192,2048]{1,0:T(8,128)(2,1)} copy(bf16[192,2048]{1,0:T(8,128)(2,1)} %shard_map.181) | data formatting | bytes 1572864
